TPU v7x, 32 devices: a whole 2x2x4 slice. The times are simulated.
32 devices in a mesh: grp: 2 (over y), ep: 4 (over z), tp: 4 (over x, core).
Axes of the slice: x: 2, y: 2, z: 4, core: 2. Of those that a mesh axis runs over, the one named last changes fastest.
Arguments:
- memory_query_rows: bfloat16 [1024, 1024], P(('grp', 'ep'), 'tp'), parts along dimension 0, may hold values from -6 to 6
- memory_key_rows: bfloat16 [1024, 1024], P(('grp', 'ep'), 'tp'), parts along dimension 0, may hold values from -6 to 6
- memory_value_rows: bfloat16 [1024, 1024], P(('grp', 'ep'), 'tp'), parts along dimension 0, may hold values from -6 to 6
- input_gate_log: float32 [8, 1024], P('tp', ('grp', 'ep')), parts along dimension 1, may hold values from -4 to 300
- forget_gate_logits: float32 [8, 1024], P('tp', ('grp', 'ep')), parts along dimension 1
- forget_log_extra: float32 [8, 1024], P('tp', ('grp', 'ep')), parts along dimension 1, may hold values from -1.5 to 0
- memory_output_weight: bfloat16 [1024, 2048], P(None, 'tp'), may hold values from -0.1875 to 0.1875
- second_batch_tokens: bfloat16 [4096, 2048], P(('grp', 'ep', 'tp')), parts along dimension 0, may hold values from -6 to 6
- expert_norm_gain: float32 [2048], replicated, may hold values from 0.1 to 1.9
- routing_expert_index: int32 [4096, 2], P(('grp', 'ep', 'tp')), parts along dimension 0, may hold values from 0 to 3, all different within a row; in each aligned block of 128 rows (0 to 127, 128 to 255, ...) at most 80 rows name the same one
- routing_expert_weight: float32 [4096, 2], P(('grp', 'ep', 'tp')), parts along dimension 0, may hold values from 0.2 to 1
- expert_gate_matrix: bfloat16 [4, 2048, 3584], P('ep', None, 'tp'), may hold values from -0.125 to 0.125
- expert_up_matrix: bfloat16 [4, 2048, 3584], P('ep', None, 'tp'), may hold values from -0.125 to 0.125
- expert_down_matrix: bfloat16 [4, 3584, 2048], P('ep', 'tp'), may hold values from -0.09375 to 0.09375
Outputs:
- mixed_out: bfloat16 [1024, 2048], P(('grp', 'ep'), 'tp'), parts along dimension 0
- expert_out: bfloat16 [4096, 2048], P(('grp', 'ep', 'tp')), parts along dimension 0
There are 2 independent parts, one for each index of `grp`. A program takes and returns all parts, laid end to end along the dimension named above; an argument that names none is the same for every part. Nothing has to cross between parts.
Inputs may be any that keep to these rules, and one draw needn't show every extreme that they name: `routing_expert_index`: within the rows of one device no expert is named by more than 80 rows, a bound that some block reaches; the 2 experts of a row differ.
All inputs are finite; a program needn't handle non-finite values.
Results may differ from a plain program's by a relative error of at most 0.012.
The roundings to bfloat16 on the way count: a program that leaves them out, or rounds other values in their place, can miss the bound.
Values may be sent and summed in bfloat16 or wider, within the bound.
A program may use at most 128 MiB of HBM per device.

v0:
```python
import functools

import jax
import jax.numpy as jnp
from jax import lax
from jax.experimental import pallas as pl
from jax.experimental.pallas import tpu as pltpu
from jax.sharding import PartitionSpec as P

DH = 128
TOP = 2
BLOCK = 128


neg_big = -1e30
rms_eps = 1e-06
highest = lax.Precision.HIGHEST


MESH = pl.DeviceIdType.MESH
LANES = 128


def expert_kernel(
    ep,
    tp,
    cap,
    out_ref,
    query_ref,
    key_ref,
    value_ref,
    in_gate_ref,
    logit_ref,
    extra_ref,
    mix_hbm,
    gate_hbm,
    up_hbm,
    down_hbm,
    ret_ref,
    mixed_ref,
    gate_up,
    down,
    rows,
    hidden,
    part,
    near_part,
    pair_sum,
    far_part,
    result,
    local_state,
    state_in,
    state_out,
    memory,
    mix,
    w_sem,
    own_sem,
    st_sem,
    z_sem,
    far_sem,
    near_sem,
    relay_sem,
    np_sem,
    fp_sem,
    r_sem,
    m_sem,
):
    e = lax.axis_index("ep")
    t = lax.axis_index("tp")
    side, core = t // 2, t % 2
    near = side * 2 + (1 - core)
    far = (1 - side) * 2 + core
    across = (1 - side) * 2 + (1 - core)
    heads = in_gate_ref.shape[0]
    length = in_gate_ref.shape[1]
    tiles = gate_up.shape[0]
    width = rows.shape[2]

    def place(side_at, core_at):
        return pl.ds(pl.multiple_of((core_at * 2 + side_at) * cap, cap), cap)

    mine = place(side, core)
    theirs = place(1 - side, core)

    def remote(src, dst, sems, k, target):
        return pltpu.make_async_remote_copy(
            src_ref=src,
            dst_ref=dst,
            send_sem=sems.at[0, k],
            recv_sem=sems.at[1, k],
            device_id=target,
            device_id_type=MESH,
        )

    def ahead(k):
        return {"ep": lax.rem(e + k, ep)}

    def behind(k):
        return {"ep": lax.rem(e + ep - k, ep)}

    def weight_copies(i):
        cols = pl.ds(pl.multiple_of(i * LANES, LANES), LANES)
        return (
            pltpu.make_async_copy(
                gate_hbm.at[0, :, cols], gate_up.at[i, :, pl.ds(0, LANES)], w_sem.at[0, i]
            ),
            pltpu.make_async_copy(
                up_hbm.at[0, :, cols], gate_up.at[i, :, pl.ds(LANES, LANES)], w_sem.at[1, i]
            ),
        )

    down_copy = pltpu.make_async_copy(down_hbm.at[0], down, own_sem.at[1])
    own_copy = pltpu.make_async_copy(out_ref.at[0], rows.at[0, mine], own_sem.at[0])

    def z_copy(k):
        return remote(out_ref.at[k], rows.at[k, mine], z_sem, k, ahead(k))

    state_copy = remote(state_out, state_in, st_sem, 0, ahead(1))
    mix_copy = pltpu.make_async_copy(mix_hbm, mix, own_sem.at[2])

    def memory_copy(i):
        span = memory.at[t]
        return remote(span, span, m_sem, i, {"tp": (near, far, across)[i]})

    def gates(h):
        logits = logit_ref[h : h + 1, :]
        forget = (
            jnp.minimum(logits, 0.0) - jnp.log1p(jnp.exp(-jnp.abs(logits)))
        ) + extra_ref[h : h + 1, :]
        at_row = lax.broadcasted_iota(jnp.int32, (length, length), 0)
        at_col = lax.broadcasted_iota(jnp.int32, (length, length), 1)
        diagonal = at_row == at_col
        in_row = in_gate_ref[h : h + 1, :]
        in_col = jnp.sum(jnp.where(diagonal, in_row, 0.0), axis=1, keepdims=True)
        sum_col = jnp.sum(jnp.where(at_col <= at_row, forget, 0.0), axis=1, keepdims=True)
        sum_row = jnp.sum(jnp.where(diagonal, sum_col, 0.0), axis=0, keepdims=True)
        total = jnp.sum(forget, axis=1, keepdims=True)
        return in_row, in_col, sum_row, sum_col, total, at_col <= at_row

    def head(ref, h):
        return ref[:, h * DH : (h + 1) * DH].astype(jnp.float32)

    def local_part():
        for h in range(heads):
            _, in_col, _, sum_col, total, _ = gates(h)
            weights = total - sum_col + in_col
            stab = jnp.max(weights, axis=0, keepdims=True)
            weighted = jnp.exp(weights - stab) * (head(key_ref, h) * DH ** (-0.5))
            local_state[h, 0:DH, :] = jnp.dot(
                weighted.T, head(value_ref, h), precision=highest,
                preferred_element_type=jnp.float32,
            )
            local_state[h, DH : DH + 1, :] = jnp.sum(weighted, axis=0, keepdims=True)
            local_state[h, DH + 1 : DH + 2, :] = jnp.broadcast_to(stab, (1, DH))
            local_state[h, DH + 2 : DH + 3, :] = jnp.broadcast_to(total, (1, DH))

    def pass_state():
        for h in range(heads):
            total = local_state[h, DH + 2 : DH + 3, :]
            stab_own = local_state[h, DH + 1 : DH + 2, :]
            carried = total + state_in[h, DH + 1 : DH + 2, :]
            stab = jnp.maximum(carried, stab_own)
            old, new = jnp.exp(carried - stab), jnp.exp(stab_own - stab)
            state_out[h, 0 : DH + 1, :] = (
                old * state_in[h, 0 : DH + 1, :] + new * local_state[h, 0 : DH + 1, :]
            )
            state_out[h, DH + 1 : DH + 2, :] = stab
        state_copy.start()

    def memory_part():
        for h in range(heads):
            in_row, _, sum_row, sum_col, _, causal = gates(h)
            decays = jnp.where(causal, sum_col - sum_row + in_row, -jnp.inf)
            carried_max = sum_col + state_in[h, DH + 1 : DH + 2, 0:1]
            row_max = jnp.maximum(jnp.max(decays, axis=1, keepdims=True), carried_max)
            queries = head(query_ref, h)
            keys = head(key_ref, h) * DH ** (-0.5)
            scores = jnp.dot(
                queries, keys.T, precision=highest, preferred_element_type=jnp.float32
            ) * jnp.exp(decays - row_max)
            carried = jnp.exp(carried_max - row_max)
            numerator = carried * jnp.dot(
                queries, state_in[h, 0:DH, :], precision=highest,
                preferred_element_type=jnp.float32,
            ) + jnp.dot(
                scores, head(value_ref, h), precision=highest,
                preferred_element_type=jnp.float32,
            )
            denominator = carried * jnp.sum(
                queries * state_in[h, DH : DH + 1, :], axis=1, keepdims=True
            ) + jnp.sum(scores, axis=1, keepdims=True)
            memory[t, :, h * DH : (h + 1) * DH] = (
                numerator / jnp.maximum(jnp.abs(denominator), jnp.exp(-row_max))
            ).astype(jnp.bfloat16)
        for i in range(3):
            memory_copy(i).start()

    def mix_part():
        mix_copy.wait()
        for i in range(3):
            memory_copy(i).wait_recv()
        total = jnp.zeros(mixed_ref.shape, jnp.float32)
        for i in range(tp):
            total = total + jnp.dot(
                memory[i], mix[i * heads * DH : (i + 1) * heads * DH, :],
                preferred_element_type=jnp.float32,
            )
        mixed_ref[...] = total.astype(jnp.bfloat16)

    def far_copy(k):
        return remote(rows.at[k, mine], rows.at[k, mine], far_sem, k, {"tp": far})

    def near_copy(k):
        return remote(rows.at[k, mine], rows.at[k, mine], near_sem, k, {"tp": near})

    def relay_copy(k):
        return remote(rows.at[k, theirs], rows.at[k, theirs], relay_sem, k, {"tp": near})

    def near_part_copy(k):
        span = pl.ds(pl.multiple_of((1 - core) * 2 * cap, 2 * cap), 2 * cap)
        return remote(part.at[k, span], near_part.at[k], np_sem, k, {"tp": near})

    def far_part_copy(k):
        return remote(pair_sum.at[k], far_part.at[k], fp_sem, k, {"tp": far})

    def return_copy(k):
        return remote(result.at[k], ret_ref.at[k], r_sem, k, behind(k))

    barrier = pltpu.get_barrier_semaphore()

    @pl.loop(1, ep)
    def _(k):
        pl.semaphore_signal(barrier, inc=1, device_id=ahead(k), device_id_type=MESH)

    for target in (near, far, across):
        pl.semaphore_signal(barrier, inc=1, device_id={"tp": target}, device_id_type=MESH)
    own_copy.start()
    pl.semaphore_wait(barrier, ep + 2)

    @pl.when(ep > 1)
    def _():
        z_copy(1).start()

    own_copy.wait()
    far_copy(0).start()
    near_copy(0).start()

    @pl.loop(0, tiles)
    def _(i):
        for copy in weight_copies(i):
            copy.start()

    down_copy.start()
    mix_copy.start()
    local_part()

    @pl.when(e == 0)
    def _():
        state_in[...] = jnp.zeros_like(state_in)
        if ep > 1:
            pass_state()

    def feed_forward(k):
        @pl.loop(0, tiles)
        def _(i):
            both = jnp.dot(rows[k], gate_up[i], preferred_element_type=jnp.float32)
            act, up_act = both[:, :LANES], both[:, LANES:]
            hidden[:, pl.ds(pl.multiple_of(i * LANES, LANES), LANES)] = (
                jax.nn.silu(act) * up_act
            ).astype(jnp.bfloat16)

        @pl.when(k == 0)
        def _():
            down_copy.wait()

        @pl.loop(0, width // 256)
        def _(i):
            cols = pl.ds(pl.multiple_of(i * 256, 256), 256)
            part[k, :, cols] = jnp.dot(
                hidden[...], down[:, cols], preferred_element_type=jnp.float32
            ).astype(jnp.bfloat16)

    def pair_stage(k):
        near_part_copy(k).wait_recv()
        other = pl.ds(pl.multiple_of((1 - side) * cap, cap), cap)
        pair_sum[k] = (
            part[k, theirs].astype(jnp.float32) + near_part[k, other].astype(jnp.float32)
        ).astype(jnp.bfloat16)
        far_part_copy(k).start()

    def final_stage(k):
        far_part_copy(k).wait_recv()
        own = pl.ds(pl.multiple_of(side * cap, cap), cap)
        total = (
            part[k, mine].astype(jnp.float32)
            + near_part[k, own].astype(jnp.float32)
            + far_part[k].astype(jnp.float32)
        ).astype(jnp.bfloat16)

        @pl.when(k == 0)
        def _():
            ret_ref[k] = total

        @pl.when(k > 0)
        def _():
            result[k] = total
            return_copy(k).start()

    @pl.loop(0, ep + 1)
    def _(k):
        @pl.when(k >= 1)
        def _():
            pair_stage(k - 1)

        @pl.when(k < ep)
        def _():
            far_copy(k).wait_recv()
            relay_copy(k).start()

        @pl.when(k + 1 < ep)
        def _():
            z_copy(k + 1).wait_recv()
            far_copy(k + 1).start()
            near_copy(k + 1).start()

        @pl.when(k + 2 < ep)
        def _():
            z_copy(k + 2).start()

        @pl.when(k == 0)
        def _():
            @pl.loop(0, tiles)
            def _(i):
                for copy in weight_copies(i):
                    copy.wait()

        @pl.when(k < ep)
        def _():
            near_copy(k).wait_recv()
            relay_copy(k).wait_recv()
            feed_forward(k)
            near_part_copy(k).start()

        @pl.when((k > 0) & (e == k))
        def _():
            state_copy.wait_recv()

            @pl.when(e + 1 < ep)
            def _():
                pass_state()

        @pl.when((k < ep) & (e == k))
        def _():
            memory_part()

        @pl.when(k >= 1)
        def _():
            final_stage(k - 1)

    mix_part()
    for i in range(3):
        memory_copy(i).wait_send()

    @pl.when(e + 1 < ep)
    def _():
        state_copy.wait_send()

    @pl.loop(0, ep)
    def _(k):
        far_copy(k).wait_send()
        near_copy(k).wait_send()
        relay_copy(k).wait_send()
        near_part_copy(k).wait_send()
        far_part_copy(k).wait_send()

    @pl.loop(1, ep)
    def _(k):
        z_copy(k).wait_send()

        return_copy(k).wait()


def expert_exchange(outgoing, memory_args, mix_weight, gate, up, down):
    ep, tp = lax.axis_size("ep"), lax.axis_size("tp")
    _, cap, width = outgoing.shape
    part_hidden = gate.shape[2]
    tiles = part_hidden // LANES
    bf16 = jnp.bfloat16
    vmem = pl.BlockSpec(memory_space=pltpu.VMEM)
    hbm = pl.BlockSpec(memory_space=pl.ANY)
    pair = pltpu.SemaphoreType.DMA((2, ep))
    rows = ep * tp * cap
    positions = memory_args[0].shape[0]
    heads = memory_args[3].shape[0]
    state = pltpu.VMEM((heads, DH + 8, DH), jnp.float32)
    return pl.pallas_call(
        functools.partial(expert_kernel, ep, tp, cap),
        out_shape=(
            jax.ShapeDtypeStruct(outgoing.shape, bf16),
            jax.ShapeDtypeStruct((positions, mix_weight.shape[1]), bf16),
        ),
        in_specs=[vmem] * 7 + [hbm] * 4,
        out_specs=(vmem, vmem),
        scratch_shapes=[
            pltpu.VMEM((tiles, width, 2 * LANES), bf16),
            pltpu.VMEM((part_hidden, width), bf16),
            pltpu.VMEM((ep, tp * cap, width), bf16),
            pltpu.VMEM((tp * cap, part_hidden), bf16),
            pltpu.VMEM((ep, tp * cap, width), bf16),
            pltpu.VMEM((ep, 2 * cap, width), bf16),
            pltpu.VMEM((ep, cap, width), bf16),
            pltpu.VMEM((ep, cap, width), bf16),
            pltpu.VMEM((ep, cap, width), bf16),
            state,
            state,
            state,
            pltpu.VMEM((tp, positions, heads * DH), bf16),
            pltpu.VMEM(mix_weight.shape, bf16),
            pltpu.SemaphoreType.DMA((2, tiles)),
            pltpu.SemaphoreType.DMA((3,)),
        ]
        + [pair] * 8
        + [pltpu.SemaphoreType.DMA((2, 3))],
        compiler_params=pltpu.CompilerParams(
            collective_id=0, has_side_effects=True, vmem_limit_bytes=66000000
        ),
        cost_estimate=pl.CostEstimate(
            flops=6 * rows * width * part_hidden, bytes_accessed=6 * width * part_hidden,
            transcendentals=rows * part_hidden,
        ),
    )(outgoing, *memory_args, mix_weight, gate, up, down)


def route_slots(routing_expert_index, experts, stride):
    flat_ids = routing_expert_index.reshape(-1)
    order = jnp.arange(flat_ids.shape[0], dtype=jnp.int32)
    earlier = (flat_ids[:, None] == flat_ids[None, :]) & (order[None, :] < order[:, None])
    route_ranks = jnp.sum(earlier.astype(jnp.int32), axis=1)
    turn = lax.rem(flat_ids + experts - lax.axis_index("ep"), experts)
    return (turn * stride + route_ranks).reshape(routing_expert_index.shape)


def on_device(
    memory_query_rows,
    memory_key_rows,
    memory_value_rows,
    input_gate_log,
    forget_gate_logits,
    forget_log_extra,
    memory_output_weight,
    second_batch_tokens,
    expert_norm_gain,
    routing_expert_index,
    routing_expert_weight,
    expert_gate_matrix,
    expert_up_matrix,
    expert_down_matrix,
):
    tok_rows = second_batch_tokens.shape[0]
    experts = lax.axis_size("ep")
    capacity = max(2, 5 * tok_rows * TOP // (4 * experts))
    stride = -(-capacity // 16) * 16
    slots_dev = experts * stride
    tokens_f = second_batch_tokens.astype(jnp.float32)
    normed = (
        tokens_f
        * lax.rsqrt(jnp.mean(tokens_f * tokens_f, axis=1, keepdims=True) + rms_eps)
        * expert_norm_gain
    ).astype(jnp.bfloat16)
    slot_ids = route_slots(routing_expert_index, experts, stride)
    slot_table = jnp.arange(slots_dev, dtype=jnp.int32)
    placing = jnp.zeros((slots_dev, tok_rows), jnp.bfloat16)
    for column in range(TOP):
        placing = placing + (slot_table[:, None] == slot_ids[None, :, column]).astype(jnp.bfloat16)
    outgoing = jnp.dot(placing, normed, preferred_element_type=jnp.float32).astype(jnp.bfloat16)
    returned, mixed_out = expert_exchange(
        outgoing.reshape(experts, stride, -1),
        (
            memory_query_rows,
            memory_key_rows,
            memory_value_rows,
            input_gate_log,
            forget_gate_logits,
            forget_log_extra,
        ),
        memory_output_weight,
        expert_gate_matrix,
        expert_up_matrix,
        expert_down_matrix,
    )
    choosing = jnp.zeros((tok_rows, slots_dev), jnp.float32)
    for column in range(TOP):
        choosing = choosing + jnp.where(
            slot_table[None, :] == slot_ids[:, column : column + 1],
            routing_expert_weight[:, column : column + 1],
            0.0,
        )
    expert_out = jnp.dot(
        choosing, returned.reshape(slots_dev, -1).astype(jnp.float32), precision=lax.Precision.HIGH
    ).astype(jnp.bfloat16)
    return (mixed_out, expert_out)


def solution(mesh):
    placed = (
        P(("grp", "ep"), "tp"),
        P(("grp", "ep"), "tp"),
        P(("grp", "ep"), "tp"),
        P("tp", ("grp", "ep")),
        P("tp", ("grp", "ep")),
        P("tp", ("grp", "ep")),
        P(None, "tp"),
        P(("grp", "ep", "tp"), None),
        P(),
        P(("grp", "ep", "tp"), None),
        P(("grp", "ep", "tp"), None),
        P("ep", None, "tp"),
        P("ep", None, "tp"),
        P("ep", "tp", None),
    )
    return jax.shard_map(
        on_device,
        mesh=mesh,
        in_specs=placed,
        out_specs=(P(("grp", "ep"), "tp"), P(("grp", "ep", "tp"), None)),
        check_vma=False,
    )
```

profile of v0, /device:TPU:0, one launch (start us, length us, event | category | flops | bytes accessed | tf_op | source)
XLA Modules:
  0.0 98.6 jit_solution(15202046631747589183)
XLA Ops:
  0.6 0.8 copy.40
  1.4 0.1 eq.72
  1.6 0.2 convert_reduce_fusion
  1.7 0.1 reduce_sum.21
  1.9 0.1 copy.41
  2.0 0.7 fusion.24
  2.7 1.2 %fusion = f32[128]{0:T(128)S(1)} fusion(bf16[128,2048]{1,0:T(8,128)(2,1)} %param.21), kind=kLoop, calls=%fused_computation.4 | loop fusion | flops 786304 | bytes 524800 | tf_op jit(solution)/shard_map/reduce_sum | solution.py:466
  3.9 2.7 %convolution_convert_fusion = bf16[320,2048]{1,0:T(8,128)(2,1)} fusion(bf16[128,2048]{1,0:T(8,128)(2,1)} %param.21, f32[2048]{0:T(1024)} %param.22, f32[128]{0:T(128)S(1)} %add_rsqrt_fusion, s32[128]{0:T(128)S(1)} %get-tuple-element.9, s32[128]{0:T(128)S(1)} %get-tuple-element.8), kind=kOutput, calls=%fused_computation | convolution fusion | flops 169803776 | bytes 1844736 | tf_op jit(solution)/shard_map/dot_general | solution.py:474
  6.6 0.0 copy-start.1
  6.6 88.4 %shard_map.149 = (bf16[4,80,2048]{2,1,0:T(8,128)(2,1)}, bf16[128,512]{1,0:T(8,128)(2,1)}) custom-call(bf16[4,80,2048]{2,1,0:T(8,128)(2,1)} %bitcast.12, bf16[128,256]{1,0:T(8,128)(2,1)} %query_ref.1, bf16[128,256]{1,0:T(8,128)(2,1)} %key_ref.1, bf16[128,256]{1,0:T(8,128)(2,1)} %value_ref.1, f32[2,128]{1,0:T(2,128)} %in_gate_ref.1, f32[2,128]{1,0:T(2,128)} %logit_ref.1, ...), custom_call_target="tpu_custom_call" | custom-call | flops 14092861440 | bytes 11010048 | tf_op jit(solution)/shard_map/pallas_call | solution.py:395
  95.0 0.0 copy-start
  95.0 0.0 copy-done.1
  95.1 2.9 %convolution_convert_fusion.1 = bf16[128,2048]{1,0:T(8,128)(2,1)} fusion(bf16[320,2048]{1,0:T(8,128)(2,1)} %bitcast.11, f32[128]{0:T(128)S(1)} %get-tuple-element.7, s32[128]{0:T(128)S(1)} %get-tuple-element.9, f32[128]{0:T(128)S(1)} %get-tuple-element.6, s32[128]{0:T(128)S(1)} %get-tuple-element.8), kind=kOutput, calls=%fused_computation.1 | convolution fusion | flops 503783424 | bytes 1837056 | tf_op jit(solution)/shard_map/dot_general | solution.py:497
  98.0 0.0 copy-done
  98.0 0.7 copy.43
  (3 shorter events, 0.0 us)
Async XLA Ops:
  6.6 88.4 %copy-start.1 = (f32[128,2]{0,1:T(2,128)S(1)}, f32[128,2]{0,1:T(2,128)}, u32[]{:S(2)}) copy-start(f32[128,2]{0,1:T(2,128)} %param.24) | copy-start | bytes 3076
  95.0 2.9 %copy-start = (bf16[128,512]{1,0:T(8,128)(2,1)S(1)}, bf16[128,512]{1,0:T(8,128)(2,1)}, u32[]{:S(2)}) copy-start(bf16[128,512]{1,0:T(8,128)(2,1)} %get-tuple-element.12) | copy-start | bytes 393220
where the time goes:
time: 98.9 us; the launch traced here: 98.6 us
  Pallas kernels  88.4 us (89%)
  matrix products  5.61 us (6%)
  other arithmetic  2.13 us (2%)
  local copies, waits for them, and re-layouts  1.8 us (2%)
    pallas_call x1, Pallas kernels, expert_exchange(): pl.pallas_call(functools.partial(expert_kernel, ep, tp, cap), out_shape=(...  88.4 us
    dot_general x1, matrix products, on_device(): jnp.dot(choosing, returned.reshape(slots_dev, -1).astype(jnp.float32), pr...  2.91 us
    dot_general x1, matrix products, on_device(): jnp.dot(placing, normed, preferred_element_type=jnp.float32)  2.7 us

commit v1 on v0

v1 whole, which is shorter than its diff:
```python
import functools

import jax
import jax.numpy as jnp
from jax import lax
from jax.experimental import pallas as pl
from jax.experimental.pallas import tpu as pltpu
from jax.sharding import PartitionSpec as P

DH = 128
TOP = 2

rms_eps = 1e-06
highest = lax.Precision.HIGHEST


MESH = pl.DeviceIdType.MESH
LANES = 128
GROUP = 16


def pieces(cap):
    half = -(-cap // 32) * 16
    return [(0, half), (half, cap - half)] if cap > half else [(0, cap)]


def fused_kernel(
    ep,
    tp,
    cap,
    query_hbm,
    key_hbm,
    value_hbm,
    in_gate_ref,
    logit_ref,
    extra_ref,
    mix_hbm,
    token_hbm,
    gain_ref,
    index_ref,
    weight_ref,
    gate_hbm,
    up_hbm,
    down_hbm,
    mixed_ref,
    out_ref,
    query_ref,
    key_ref,
    value_ref,
    tokens,
    normed,
    send,
    slot_row,
    slot_col,
    weight_col,
    gate_up,
    down,
    rows,
    hidden,
    part,
    near_part,
    pair_sum,
    far_part,
    result,
    returned,
    total_out,
    local_state,
    state_in,
    state_out,
    memory,
    mix,
    w_sem,
    own_sem,
    st_sem,
    z_sem,
    far_sem,
    near_sem,
    relay_sem,
    no_sem,
    nf_sem,
    fp_sem,
    r_sem,
    m_sem,
    go_sem,
):
    e = lax.axis_index("ep")
    t = lax.axis_index("tp")
    side, core = t // 2, t % 2
    near = side * 2 + (1 - core)
    far = (1 - side) * 2 + core
    across = (1 - side) * 2 + (1 - core)
    heads = in_gate_ref.shape[0]
    length = in_gate_ref.shape[1]
    tiles = gate_up.shape[0]
    width = rows.shape[2]
    tok_rows = tokens.shape[0]
    cuts = pieces(cap)
    count = range(len(cuts))
    line = ep == 4

    if line:
        left = 1 - e // 2
        inner = e * left + (3 - e) * (1 - left)

        def seat(v):
            return v * left + (3 - v) * (1 - left)

        targets = [e, seat(1 + 2 * inner), seat(3 - inner), seat(2 - 2 * inner)]
        sources = [e, targets[3], targets[2], targets[1]]
        gathers = [e, seat(3), seat(2), seat(1 - inner)]
    else:
        targets = [lax.rem(e + k, ep) for k in range(ep)]
        sources = [lax.rem(e + ep - k, ep) for k in range(ep)]
        gathers = targets

    def block(side_at, core_at, p=None):
        off, size = (0, cap) if p is None else cuts[p]
        return pl.ds(pl.multiple_of((side_at * 2 + core_at) * cap + off, GROUP), size)

    def cut(p):
        return pl.ds(cuts[p][0], cuts[p][1])

    def remote(src, dst, sent, received, target):
        return pltpu.make_async_remote_copy(
            src_ref=src,
            dst_ref=dst,
            send_sem=sent,
            recv_sem=received,
            device_id=target,
            device_id_type=MESH,
        )

    def weight_copies(i):
        cols = pl.ds(pl.multiple_of(i * LANES, LANES), LANES)
        return (
            pltpu.make_async_copy(
                gate_hbm.at[0, :, cols], gate_up.at[i, :, pl.ds(0, LANES)], w_sem.at[0, i]
            ),
            pltpu.make_async_copy(
                up_hbm.at[0, :, cols], gate_up.at[i, :, pl.ds(LANES, LANES)], w_sem.at[1, i]
            ),
        )

    token_copy = pltpu.make_async_copy(token_hbm, tokens, own_sem.at[0])
    down_copy = pltpu.make_async_copy(down_hbm.at[0], down, own_sem.at[1])
    mix_copy = pltpu.make_async_copy(mix_hbm, mix, own_sem.at[2])
    head_copies = [
        pltpu.make_async_copy(query_hbm, query_ref, own_sem.at[3]),
        pltpu.make_async_copy(key_hbm, key_ref, own_sem.at[4]),
        pltpu.make_async_copy(value_hbm, value_ref, own_sem.at[5]),
    ]

    def z_send(s, p):
        return remote(
            send.at[s, cut(p)], rows.at[e, block(side, core, p)],
            z_sem.at[0, s, p], z_sem.at[1, e, p], {"ep": s},
        )

    def z_recv(s, p):
        return remote(
            send.at[s, cut(p)], rows.at[s, block(side, core, p)],
            z_sem.at[0, s, p], z_sem.at[1, s, p], {"ep": s},
        )

    def mine_copy(s, p, sems, target):
        span = rows.at[s, block(side, core, p)]
        return remote(span, span, sems.at[0, s, p], sems.at[1, s, p], {"tp": target})

    def far_copy(s, p):
        return mine_copy(s, p, far_sem, far)

    def near_copy(s, p):
        return mine_copy(s, p, near_sem, near)

    def relay_copy(s, p):
        span = rows.at[s, block(1 - side, core, p)]
        return remote(span, span, relay_sem.at[0, s, p], relay_sem.at[1, s, p], {"tp": near})

    def near_own_copy(s):
        return remote(
            part.at[s, block(side, 1 - core)], near_part.at[s, 0],
            no_sem.at[0, s], no_sem.at[1, s], {"tp": near},
        )

    def near_far_copy(s):
        return remote(
            part.at[s, block(1 - side, 1 - core)], near_part.at[s, 1],
            nf_sem.at[0, s], nf_sem.at[1, s], {"tp": near},
        )

    def far_part_copy(s, p):
        return remote(
            pair_sum.at[s, cut(p)], far_part.at[s, cut(p)],
            fp_sem.at[0, s, p], fp_sem.at[1, s, p], {"tp": far},
        )

    def return_send(s, p):
        return remote(
            result.at[s, cut(p)], returned.at[e, cut(p)],
            r_sem.at[0, s, p], r_sem.at[1, e, p], {"ep": s},
        )

    def return_recv(s, p):
        return remote(
            result.at[s, cut(p)], returned.at[s, cut(p)],
            r_sem.at[0, s, p], r_sem.at[1, s, p], {"ep": s},
        )

    state_copy = remote(
        state_out, state_in, st_sem.at[0, 0], st_sem.at[1, 0], {"ep": lax.rem(e + 1, ep)}
    )

    def memory_copy(i):
        span = memory.at[far if i == 2 else t]
        return remote(
            span, span, m_sem.at[0, i], m_sem.at[1, i], {"tp": far if i == 1 else near}
        )

    def gates(h):
        logits = logit_ref[h : h + 1, :]
        forget = (
            jnp.minimum(logits, 0.0) - jnp.log1p(jnp.exp(-jnp.abs(logits)))
        ) + extra_ref[h : h + 1, :]
        at_row = lax.broadcasted_iota(jnp.int32, (length, length), 0)
        at_col = lax.broadcasted_iota(jnp.int32, (length, length), 1)
        diagonal = at_row == at_col
        in_row = in_gate_ref[h : h + 1, :]
        in_col = jnp.sum(jnp.where(diagonal, in_row, 0.0), axis=1, keepdims=True)
        sum_col = jnp.sum(jnp.where(at_col <= at_row, forget, 0.0), axis=1, keepdims=True)
        sum_row = jnp.sum(jnp.where(diagonal, sum_col, 0.0), axis=0, keepdims=True)
        total = jnp.sum(forget, axis=1, keepdims=True)
        return in_row, in_col, sum_row, sum_col, total, at_col <= at_row

    def head(ref, h):
        return ref[:, h * DH : (h + 1) * DH].astype(jnp.float32)

    def local_part():
        for h in range(heads):
            _, in_col, _, sum_col, total, _ = gates(h)
            weights = total - sum_col + in_col
            stab = jnp.max(weights, axis=0, keepdims=True)
            weighted = jnp.exp(weights - stab) * (head(key_ref, h) * DH ** (-0.5))
            local_state[h, 0:DH, :] = jnp.dot(
                weighted.T, head(value_ref, h), precision=highest,
                preferred_element_type=jnp.float32,
            )
            local_state[h, DH : DH + 1, :] = jnp.sum(weighted, axis=0, keepdims=True)
            local_state[h, DH + 1 : DH + 2, :] = jnp.broadcast_to(stab, (1, DH))
            local_state[h, DH + 2 : DH + 3, :] = jnp.broadcast_to(total, (1, DH))

    def pass_state():
        for h in range(heads):
            total = local_state[h, DH + 2 : DH + 3, :]
            stab_own = local_state[h, DH + 1 : DH + 2, :]
            carried = total + state_in[h, DH + 1 : DH + 2, :]
            stab = jnp.maximum(carried, stab_own)
            old, new = jnp.exp(carried - stab), jnp.exp(stab_own - stab)
            state_out[h, 0 : DH + 1, :] = (
                old * state_in[h, 0 : DH + 1, :] + new * local_state[h, 0 : DH + 1, :]
            )
            state_out[h, DH + 1 : DH + 2, :] = stab
        state_copy.start()

    def memory_part():
        for h in range(heads):
            in_row, _, sum_row, sum_col, _, causal = gates(h)
            decays = jnp.where(causal, sum_col - sum_row + in_row, -jnp.inf)
            carried_max = sum_col + state_in[h, DH + 1 : DH + 2, 0:1]
            row_max = jnp.maximum(jnp.max(decays, axis=1, keepdims=True), carried_max)
            queries = head(query_ref, h)
            keys = head(key_ref, h) * DH ** (-0.5)
            scores = jnp.dot(
                queries, keys.T, precision=highest, preferred_element_type=jnp.float32
            ) * jnp.exp(decays - row_max)
            carried = jnp.exp(carried_max - row_max)
            numerator = carried * jnp.dot(
                queries, state_in[h, 0:DH, :], precision=highest,
                preferred_element_type=jnp.float32,
            ) + jnp.dot(
                scores, head(value_ref, h), precision=highest,
                preferred_element_type=jnp.float32,
            )
            denominator = carried * jnp.sum(
                queries * state_in[h, DH : DH + 1, :], axis=1, keepdims=True
            ) + jnp.sum(scores, axis=1, keepdims=True)
            memory[t, :, h * DH : (h + 1) * DH] = (
                numerator / jnp.maximum(jnp.abs(denominator), jnp.exp(-row_max))
            ).astype(jnp.bfloat16)
        memory_copy(0).start()
        memory_copy(1).start()

    def mix_part():
        memory_copy(1).wait_recv()
        memory_copy(2).start()
        mix_copy.wait()
        memory_copy(0).wait_recv()
        memory_copy(2).wait_recv()
        total = jnp.zeros(mixed_ref.shape, jnp.float32)
        for i in range(tp):
            total = total + jnp.dot(
                memory[i], mix[i * heads * DH : (i + 1) * heads * DH, :],
                preferred_element_type=jnp.float32,
            )
        mixed_ref[...] = total.astype(jnp.bfloat16)

    def slots():
        at_row = lax.broadcasted_iota(jnp.int32, (tok_rows, tok_rows), 0)
        at_col = lax.broadcasted_iota(jnp.int32, (tok_rows, tok_rows), 1)
        chosen = [index_ref[c : c + 1, :] == at_row for c in range(TOP)]
        member = jnp.zeros((tok_rows, tok_rows), jnp.float32)
        weights = jnp.zeros((tok_rows, tok_rows), jnp.float32)
        for c in range(TOP):
            member = member + jnp.where(chosen[c], 1.0, 0.0)
            weights = weights + jnp.where(chosen[c], weight_ref[c : c + 1, :], 0.0)
        earlier = jnp.where(at_row < at_col, 1.0, 0.0).astype(jnp.bfloat16)
        ranks = jnp.dot(member.astype(jnp.bfloat16), earlier, preferred_element_type=jnp.float32)
        slot = jnp.where(member > 0.0, ranks, -1.0)
        slot_row[...] = slot
        slot_col[...] = slot.T
        weight_col[...] = weights.T

    def norm():
        @pl.loop(0, tok_rows // GROUP)
        def _(i):
            span = pl.ds(pl.multiple_of(i * GROUP, GROUP), GROUP)
            values = tokens[span].astype(jnp.float32)
            scale = lax.rsqrt(jnp.mean(values * values, axis=1, keepdims=True) + rms_eps)
            normed[span] = (values * scale * gain_ref[...]).astype(jnp.bfloat16)

    def dispatch(x, place):
        at_slot = lax.broadcasted_iota(jnp.int32, (cap, tok_rows), 0).astype(jnp.float32)
        taken = jnp.where(at_slot == slot_row[pl.ds(x, 1), :], 1.0, 0.0).astype(jnp.bfloat16)

        @pl.loop(0, width // 512)
        def _(i):
            cols = pl.ds(pl.multiple_of(i * 512, 512), 512)
            place[:, cols] = jnp.dot(
                taken, normed[:, cols], preferred_element_type=jnp.float32
            ).astype(jnp.bfloat16)

    def combine(x, first, last):
        lane = lax.broadcasted_iota(jnp.int32, (tok_rows, tok_rows), 1)
        slot = jnp.sum(jnp.where(lane == x, slot_col[...], 0.0), axis=1, keepdims=True)
        weight = jnp.sum(jnp.where(lane == x, weight_col[...], 0.0), axis=1, keepdims=True)
        at_slot = lax.broadcasted_iota(jnp.int32, (tok_rows, cap), 1).astype(jnp.float32)
        taken = jnp.where(at_slot == slot, 1.0, 0.0).astype(jnp.bfloat16)

        @pl.loop(0, width // 512)
        def _(i):
            cols = pl.ds(pl.multiple_of(i * 512, 512), 512)
            total = weight * jnp.dot(
                taken, returned[x, :, cols], preferred_element_type=jnp.float32
            )
            if not first:
                total = total + total_out[:, cols]
            if last:
                out_ref[:, cols] = total.astype(jnp.bfloat16)
            else:
                total_out[:, cols] = total

    def feed_forward(s, group, first=False):
        span = pl.ds(pl.multiple_of(group * 2 * cap, 2 * cap), 2 * cap)

        @pl.loop(0, tiles)
        def _(i):
            if first:
                for copy in weight_copies(i):
                    copy.wait()
            both = jnp.dot(rows[s, span], gate_up[i], preferred_element_type=jnp.float32)
            act, up_act = both[:, :LANES], both[:, LANES:]
            hidden[:, pl.ds(pl.multiple_of(i * LANES, LANES), LANES)] = (
                jax.nn.silu(act) * up_act
            ).astype(jnp.bfloat16)

        if first:
            down_copy.wait()

        @pl.loop(0, width // 256)
        def _(i):
            cols = pl.ds(pl.multiple_of(i * 256, 256), 256)
            part[s, span, cols] = jnp.dot(
                hidden[...], down[:, cols], preferred_element_type=jnp.float32
            ).astype(jnp.bfloat16)

    def gather_start(s, p):
        far_copy(s, p).start()
        near_copy(s, p).start()

    def arrive(j, which=None):
        for p in count if which is None else which:
            z_recv(sources[j], p).wait_recv()
            gather_start(sources[j], p)

    def own_group(j):
        s = sources[j]
        for p in count:
            near_copy(s, p).wait_recv()
        feed_forward(s, side, first=j == 0)
        near_own_copy(s).start()

    def relay(j):
        s = sources[j]
        for p in count:
            far_copy(s, p).wait_recv()
            relay_copy(s, p).start()

    def far_group(j):
        s = sources[j]
        for p in count:
            relay_copy(s, p).wait_recv()
        feed_forward(s, 1 - side)
        near_far_copy(s).start()

    def pair(j):
        s = sources[j]
        near_far_copy(s).wait_recv()
        base = (1 - side) * 2 * cap + core * cap
        for p in count:
            off, size = cuts[p]

            @pl.loop(0, size // GROUP)
            def _(i):
                at = pl.multiple_of(off + i * GROUP, GROUP)
                pair_sum[s, pl.ds(at, GROUP)] = (
                    part[s, pl.ds(pl.multiple_of(base + at, GROUP), GROUP)].astype(jnp.float32)
                    + near_part[s, 1, pl.ds(at, GROUP)].astype(jnp.float32)
                ).astype(jnp.bfloat16)

            far_part_copy(s, p).start()

    def finish(j, which=None):
        s = sources[j]
        base = side * 2 * cap + core * cap
        for p in count if which is None else which:
            if p == 0:
                near_own_copy(s).wait_recv()
            far_part_copy(s, p).wait_recv()
            off, size = cuts[p]

            @pl.loop(0, size // GROUP)
            def _(i):
                at = pl.multiple_of(off + i * GROUP, GROUP)
                total = (
                    part[s, pl.ds(pl.multiple_of(base + at, GROUP), GROUP)].astype(jnp.float32)
                    + near_part[s, 0, pl.ds(at, GROUP)].astype(jnp.float32)
                    + far_part[s, pl.ds(at, GROUP)].astype(jnp.float32)
                ).astype(jnp.bfloat16)
                if j == 0:
                    returned[s, pl.ds(at, GROUP)] = total
                else:
                    result[s, pl.ds(at, GROUP)] = total

            if j > 0:
                return_send(s, p).start()

    def gather_back(k):
        x = gathers[k]
        if k > 0:
            for p in count:
                return_recv(x, p).wait_recv()
        combine(x, k == 0, k == ep - 1)

    def start_send(k):
        for p in count:
            z_send(targets[k], p).start()

    def state_step():
        state_copy.wait_recv()

        @pl.when(e + 1 < ep)
        def _():
            pass_state()

    token_copy.start()
    for copy in head_copies:
        copy.start()

    @pl.loop(0, tiles)
    def _(i):
        for copy in weight_copies(i):
            copy.start()

    down_copy.start()
    mix_copy.start()
    barrier = pltpu.get_barrier_semaphore()

    @pl.loop(1, ep)
    def _(k):
        pl.semaphore_signal(
            barrier, inc=1, device_id={"ep": lax.rem(e + k, ep)}, device_id_type=MESH
        )

    for target in (near, far, across):
        pl.semaphore_signal(barrier, inc=1, device_id={"tp": target}, device_id_type=MESH)
    slots()
    token_copy.wait()
    norm()
    dispatch(e, rows.at[e, block(side, core)])
    pl.semaphore_wait(barrier, ep + 2)
    for p in count:
        gather_start(e, p)
    for k in range(1, ep):
        dispatch(targets[k], send.at[targets[k]])
        if k == 1 or not line:
            start_send(k)
        elif k == 2:
            pl.when(inner == 0)(functools.partial(start_send, 2))
    for copy in head_copies:
        copy.wait()
    local_part()

    @pl.when(e == 0)
    def _():
        state_in[...] = jnp.zeros_like(state_in)
        if ep > 1:
            pass_state()

    own_group(0)
    if line:
        arrive(1)
        relay(0)
        far_group(0)
        own_group(1)

        @pl.when(inner == 0)
        def _():
            arrive(2, count[:1])
            pl.semaphore_signal(
                go_sem, inc=1, device_id={"ep": lax.rem(e + 2, ep)}, device_id_type=MESH
            )
            arrive(2, count[1:])
            start_send(3)

        @pl.when(inner == 1)
        def _():
            pair(0)
            pl.semaphore_wait(go_sem, 1)
            start_send(2)
            start_send(3)

        relay(1)
        far_group(1)

        @pl.when(inner == 1)
        def _():
            arrive(2)
            pl.when(e == 1)(state_step)

        own_group(2)

        @pl.when(inner == 0)
        def _():
            pair(1)
            relay(2)

        @pl.when(inner == 1)
        def _():
            arrive(3, count[:1])
            relay(2)
            arrive(3, count[1:])

        far_group(2)

        @pl.when(inner == 0)
        def _():
            finish(1, count[:1])
            pair(2)
            arrive(3)
            finish(1, count[1:])

        own_group(3)

        @pl.when(inner == 0)
        def _():
            finish(2)
            pair(0)
            pl.when(e == ep - 1)(state_step)
            relay(3)

        @pl.when(inner == 1)
        def _():
            pair(2)
            finish(0)
            pl.when(e == 2)(state_step)
            relay(3)

        far_group(3)

        @pl.when(inner == 0)
        def _():
            pair(3)

        @pl.when(inner == 1)
        def _():
            finish(2, count[:1])
            pair(3)
            pair(1)
            finish(2, count[1:])

        memory_part()

        @pl.when(inner == 0)
        def _():
            finish(0)
            finish(3)

        @pl.when(inner == 1)
        def _():
            finish(3)
            finish(1)

        gather_back(0)
        gather_back(1)
        mix_part()
        gather_back(2)
        gather_back(3)
    else:
        for j in range(ep):
            if j + 1 < ep:
                arrive(j + 1)
            if j > 0:
                own_group(j)
            relay(j)
            far_group(j)
            if j > 0:
                pl.when(e == j)(state_step)
            pair(j)
            if j > 0:
                finish(j - 1)
        finish(ep - 1)
        memory_part()
        mix_part()
        for k in range(ep):
            gather_back(k)

    for i in range(3):
        memory_copy(i).wait_send()

    @pl.when(e + 1 < ep)
    def _():
        state_copy.wait_send()

    @pl.loop(0, ep)
    def _(s):
        near_own_copy(s).wait_send()
        near_far_copy(s).wait_send()
        for p in count:
            far_copy(s, p).wait_send()
            near_copy(s, p).wait_send()
            relay_copy(s, p).wait_send()
            far_part_copy(s, p).wait_send()

    @pl.loop(1, ep)
    def _(k):
        s = lax.rem(e + k, ep)
        for p in count:
            z_send(s, p).wait_send()
            return_send(s, p).wait_send()


def on_device(
    memory_query_rows,
    memory_key_rows,
    memory_value_rows,
    input_gate_log,
    forget_gate_logits,
    forget_log_extra,
    memory_output_weight,
    second_batch_tokens,
    expert_norm_gain,
    routing_expert_index,
    routing_expert_weight,
    expert_gate_matrix,
    expert_up_matrix,
    expert_down_matrix,
):
    ep, tp = lax.axis_size("ep"), lax.axis_size("tp")
    tok_rows, width = second_batch_tokens.shape
    capacity = max(2, 5 * tok_rows * TOP // (4 * ep))
    cap = -(-capacity // GROUP) * GROUP
    part_hidden = expert_gate_matrix.shape[2]
    tiles = part_hidden // LANES
    positions = memory_query_rows.shape[0]
    heads = input_gate_log.shape[0]
    bf16 = jnp.bfloat16
    vmem = pl.BlockSpec(memory_space=pltpu.VMEM)
    hbm = pl.BlockSpec(memory_space=pl.ANY)
    whole = pltpu.SemaphoreType.DMA((2, ep))
    split = pltpu.SemaphoreType.DMA((2, ep, len(pieces(cap))))
    state = pltpu.VMEM((heads, DH + 8, DH), jnp.float32)
    square = pltpu.VMEM((tok_rows, tok_rows), jnp.float32)
    slotted = pltpu.VMEM((ep, cap, width), bf16)
    head_rows = pltpu.VMEM(memory_query_rows.shape, bf16)
    token_rows = pltpu.VMEM((tok_rows, width), bf16)
    return pl.pallas_call(
        functools.partial(fused_kernel, ep, tp, cap),
        out_shape=(
            jax.ShapeDtypeStruct((positions, memory_output_weight.shape[1]), bf16),
            jax.ShapeDtypeStruct((tok_rows, width), bf16),
        ),
        in_specs=[hbm] * 3 + [vmem] * 3 + [hbm] * 2 + [vmem] * 3 + [hbm] * 3,
        out_specs=(vmem, vmem),
        scratch_shapes=[
            head_rows,
            head_rows,
            head_rows,
            token_rows,
            token_rows,
            slotted,
            square,
            square,
            square,
            pltpu.VMEM((tiles, width, 2 * LANES), bf16),
            pltpu.VMEM((part_hidden, width), bf16),
            pltpu.VMEM((ep, tp * cap, width), bf16),
            pltpu.VMEM((2 * cap, part_hidden), bf16),
            pltpu.VMEM((ep, tp * cap, width), bf16),
            pltpu.VMEM((ep, 2, cap, width), bf16),
            slotted,
            slotted,
            slotted,
            slotted,
            pltpu.VMEM((tok_rows, width), jnp.float32),
            state,
            state,
            state,
            pltpu.VMEM((tp, positions, heads * DH), bf16),
            pltpu.VMEM(memory_output_weight.shape, bf16),
            pltpu.SemaphoreType.DMA((2, tiles)),
            pltpu.SemaphoreType.DMA((6,)),
            pltpu.SemaphoreType.DMA((2, 1)),
            split,
            split,
            split,
            split,
            whole,
            whole,
            split,
            split,
            pltpu.SemaphoreType.DMA((2, 3)),
            pltpu.SemaphoreType.REGULAR,
        ],
        compiler_params=pltpu.CompilerParams(
            collective_id=0, has_side_effects=True, vmem_limit_bytes=66000000
        ),
        cost_estimate=pl.CostEstimate(
            flops=6 * ep * tp * cap * width * part_hidden,
            bytes_accessed=6 * width * part_hidden,
            transcendentals=ep * tp * cap * part_hidden,
        ),
    )(
        memory_query_rows,
        memory_key_rows,
        memory_value_rows,
        input_gate_log,
        forget_gate_logits,
        forget_log_extra,
        memory_output_weight,
        second_batch_tokens,
        expert_norm_gain.reshape(1, -1),
        routing_expert_index.T,
        routing_expert_weight.T,
        expert_gate_matrix,
        expert_up_matrix,
        expert_down_matrix,
    )


def solution(mesh):
    placed = (
        P(("grp", "ep"), "tp"),
        P(("grp", "ep"), "tp"),
        P(("grp", "ep"), "tp"),
        P("tp", ("grp", "ep")),
        P("tp", ("grp", "ep")),
        P("tp", ("grp", "ep")),
        P(None, "tp"),
        P(("grp", "ep", "tp"), None),
        P(),
        P(("grp", "ep", "tp"), None),
        P(("grp", "ep", "tp"), None),
        P("ep", None, "tp"),
        P("ep", None, "tp"),
        P("ep", "tp", None),
    )
    return jax.shard_map(
        on_device,
        mesh=mesh,
        in_specs=placed,
        out_specs=(P(("grp", "ep"), "tp"), P(("grp", "ep", "tp"), None)),
        check_vma=False,
    )
```

time: 98.9 us -> 97.2 us (0.983)
  matrix products: 5.61 us -> 0 us
  Pallas kernels: 88.4 us -> 92.9 us
  other arithmetic: 2.13 us -> 0 us
  local copies, waits for them, and re-layouts: 1.8 us -> 3.45 us
    dot_general x2 -> x0, matrix products: 5.61 us -> none  [the longest x1 2.91 us: on_device(): jnp.dot(choosing, returned.reshape(slots_dev, -1).astype(jnp.float32), pr...]
    pallas_call x1, Pallas kernels: 88.4 us -> 92.9 us  [on_device(): pl.pallas_call(functools.partial(fused_kernel, ep, tp, cap), out_shape=(j...]
    unnamed x6 -> x2, local copies, waits for them, and re-layouts: 1.45 us -> 3.45 us
    reduce_sum x2 -> x0, other arithmetic: 1.41 us -> none  [the longest x1 1.23 us: on_device(): jnp.mean(tokens_f * tokens_f, axis=1, keepdims=True) + rms_eps]
where the time goes in v1:
time: 97.2 us; the launch traced here: 97 us
  Pallas kernels  92.9 us (96%)
  local copies, waits for them, and re-layouts  3.45 us (4%)
    pallas_call x1, Pallas kernels, on_device(): pl.pallas_call(functools.partial(fused_kernel, ep, tp, cap), out_shape=(j...  92.9 us
    unnamed x2, local copies, waits for them, and re-layouts  3.45 us

profile of v1, /device:TPU:0, one launch (start us, length us, event | category | flops | bytes accessed | tf_op | source)
XLA Modules:
  0.0 97.0 jit_solution(4880101309118059824)
XLA Ops:
  0.6 92.9 %shard_map.149 = (bf16[128,512]{1,0:T(8,128)(2,1)}, bf16[128,2048]{1,0:T(8,128)(2,1)}) custom-call(bf16[128,256]{1,0:T(8,128)(2,1)} %query_hbm.1, bf16[128,256]{1,0:T(8,128)(2,1)} %key_hbm.1, bf16[128,256]{1,0:T(8,128)(2,1)} %value_hbm.1, f32[2,128]{1,0:T(2,128)} %in_gate_ref.1, f32[2,128]{1,0:T(2,128)} %logit_ref.1, f32[2,128]{1,0:T(2,128)} %extra_ref.1, ...), custom_call_target="tpu_custom_call" | custom-call | flops 14092861440 | bytes 11010048 | tf_op jit(solution)/shard_map/pallas_call | solution.py:695
  93.6 1.6 %copy.18 = bf16[128,512]{1,0:T(8,128)(2,1)} copy(bf16[128,512]{1,0:T(8,128)(2,1)} %get-tuple-element.4) | data formatting | bytes 262144
  95.1 1.9 %copy.19 = bf16[128,2048]{1,0:T(8,128)(2,1)} copy(bf16[128,2048]{1,0:T(8,128)(2,1)} %get-tuple-element.5) | data formatting | bytes 1048576

commit v2 on v1

--- a/solution.py
+++ b/solution.py
@@ -20,8 +20,8 @@
 
 
 def pieces(cap):
-    half = -(-cap // 32) * 16
-    return [(0, half), (half, cap - half)] if cap > half else [(0, cap)]
+    first = cap // 32 * 16
+    return [(0, first), (first, cap - first)] if first else [(0, cap)]
 
 
 def fused_kernel(
@@ -91,11 +91,13 @@
     across = (1 - side) * 2 + (1 - core)
     heads = in_gate_ref.shape[0]
     length = in_gate_ref.shape[1]
-    tiles = gate_up.shape[0]
+    tiles = gate_up.shape[1] // (2 * LANES)
     width = rows.shape[2]
+    part_hidden = down.shape[0]
     tok_rows = tokens.shape[0]
     cuts = pieces(cap)
     count = range(len(cuts))
+    head, tail = count[:1], count[1:]
     line = ep == 4
 
     if line:
@@ -107,11 +109,17 @@
 
         targets = [e, seat(1 + 2 * inner), seat(3 - inner), seat(2 - 2 * inner)]
         sources = [e, targets[3], targets[2], targets[1]]
+
+        def source(j):
+            return sources[j]
+
         gathers = [e, seat(3), seat(2), seat(1 - inner)]
     else:
         targets = [lax.rem(e + k, ep) for k in range(ep)]
-        sources = [lax.rem(e + ep - k, ep) for k in range(ep)]
         gathers = targets
+
+        def source(j):
+            return lax.rem(e + ep - j, ep)
 
     def block(side_at, core_at, p=None):
         off, size = (0, cap) if p is None else cuts[p]
@@ -130,14 +138,17 @@
             device_id_type=MESH,
         )
 
+    def pair_cols(i, which):
+        return pl.ds(pl.multiple_of((2 * i + which) * LANES, LANES), LANES)
+
     def weight_copies(i):
         cols = pl.ds(pl.multiple_of(i * LANES, LANES), LANES)
         return (
             pltpu.make_async_copy(
-                gate_hbm.at[0, :, cols], gate_up.at[i, :, pl.ds(0, LANES)], w_sem.at[0, i]
+                gate_hbm.at[0, :, cols], gate_up.at[:, pair_cols(i, 0)], w_sem.at[0, i]
             ),
             pltpu.make_async_copy(
-                up_hbm.at[0, :, cols], gate_up.at[i, :, pl.ds(LANES, LANES)], w_sem.at[1, i]
+                up_hbm.at[0, :, cols], gate_up.at[:, pair_cols(i, 1)], w_sem.at[1, i]
             ),
         )
 
@@ -231,7 +242,7 @@
         total = jnp.sum(forget, axis=1, keepdims=True)
         return in_row, in_col, sum_row, sum_col, total, at_col <= at_row
 
-    def head(ref, h):
+    def heads_of(ref, h):
         return ref[:, h * DH : (h + 1) * DH].astype(jnp.float32)
 
     def local_part():
@@ -239,9 +250,9 @@
             _, in_col, _, sum_col, total, _ = gates(h)
             weights = total - sum_col + in_col
             stab = jnp.max(weights, axis=0, keepdims=True)
-            weighted = jnp.exp(weights - stab) * (head(key_ref, h) * DH ** (-0.5))
+            weighted = jnp.exp(weights - stab) * (heads_of(key_ref, h) * DH ** (-0.5))
             local_state[h, 0:DH, :] = jnp.dot(
-                weighted.T, head(value_ref, h), precision=highest,
+                weighted.T, heads_of(value_ref, h), precision=highest,
                 preferred_element_type=jnp.float32,
             )
             local_state[h, DH : DH + 1, :] = jnp.sum(weighted, axis=0, keepdims=True)
@@ -267,8 +278,8 @@
             decays = jnp.where(causal, sum_col - sum_row + in_row, -jnp.inf)
             carried_max = sum_col + state_in[h, DH + 1 : DH + 2, 0:1]
             row_max = jnp.maximum(jnp.max(decays, axis=1, keepdims=True), carried_max)
-            queries = head(query_ref, h)
-            keys = head(key_ref, h) * DH ** (-0.5)
+            queries = heads_of(query_ref, h)
+            keys = heads_of(key_ref, h) * DH ** (-0.5)
             scores = jnp.dot(
                 queries, keys.T, precision=highest, preferred_element_type=jnp.float32
             ) * jnp.exp(decays - row_max)
@@ -277,7 +288,7 @@
                 queries, state_in[h, 0:DH, :], precision=highest,
                 preferred_element_type=jnp.float32,
             ) + jnp.dot(
-                scores, head(value_ref, h), precision=highest,
+                scores, heads_of(value_ref, h), precision=highest,
                 preferred_element_type=jnp.float32,
             )
             denominator = carried * jnp.sum(
@@ -360,62 +371,65 @@
 
     def feed_forward(s, group, first=False):
         span = pl.ds(pl.multiple_of(group * 2 * cap, 2 * cap), 2 * cap)
-
-        @pl.loop(0, tiles)
-        def _(i):
+        step = 4 * LANES
+        for start in range(0, 2 * part_hidden, step):
+            stop = min(start + step, 2 * part_hidden)
             if first:
-                for copy in weight_copies(i):
-                    copy.wait()
-            both = jnp.dot(rows[s, span], gate_up[i], preferred_element_type=jnp.float32)
-            act, up_act = both[:, :LANES], both[:, LANES:]
-            hidden[:, pl.ds(pl.multiple_of(i * LANES, LANES), LANES)] = (
-                jax.nn.silu(act) * up_act
-            ).astype(jnp.bfloat16)
-
+                for i in range(start // (2 * LANES), stop // (2 * LANES)):
+                    for copy in weight_copies(i):
+                        copy.wait()
+            both = jnp.dot(
+                rows[s, span], gate_up[:, start:stop], preferred_element_type=jnp.float32
+            )
+            for i in range(0, stop - start, 2 * LANES):
+                act, up_act = both[:, i : i + LANES], both[:, i + LANES : i + 2 * LANES]
+                at = (start + i) // 2
+                hidden[:, at : at + LANES] = (jax.nn.silu(act) * up_act).astype(jnp.bfloat16)
         if first:
             down_copy.wait()
-
-        @pl.loop(0, width // 256)
-        def _(i):
-            cols = pl.ds(pl.multiple_of(i * 256, 256), 256)
-            part[s, span, cols] = jnp.dot(
-                hidden[...], down[:, cols], preferred_element_type=jnp.float32
-            ).astype(jnp.bfloat16)
+        part[s, span] = jnp.dot(
+            hidden[...], down[...], preferred_element_type=jnp.float32
+        ).astype(jnp.bfloat16)
 
     def gather_start(s, p):
         far_copy(s, p).start()
         near_copy(s, p).start()
 
+    def land(j):
+        for p in count:
+            z_recv(source(j), p).wait_recv()
+
     def arrive(j, which=None):
         for p in count if which is None else which:
-            z_recv(sources[j], p).wait_recv()
-            gather_start(sources[j], p)
-
-    def own_group(j):
-        s = sources[j]
+            z_recv(source(j), p).wait_recv()
+            gather_start(source(j), p)
+
+    def own_group(j, first=False):
+        s = source(j)
         for p in count:
             near_copy(s, p).wait_recv()
-        feed_forward(s, side, first=j == 0)
+        feed_forward(s, side, first=first)
         near_own_copy(s).start()
 
     def relay(j):
-        s = sources[j]
+        s = source(j)
         for p in count:
             far_copy(s, p).wait_recv()
             relay_copy(s, p).start()
 
     def far_group(j):
-        s = sources[j]
+        s = source(j)
         for p in count:
             relay_copy(s, p).wait_recv()
         feed_forward(s, 1 - side)
         near_far_copy(s).start()
 
-    def pair(j):
-        s = sources[j]
-        near_far_copy(s).wait_recv()
+    def pair(j, which=None):
+        s = source(j)
         base = (1 - side) * 2 * cap + core * cap
-        for p in count:
+        for p in count if which is None else which:
+            if p == 0:
+                near_far_copy(s).wait_recv()
             off, size = cuts[p]
 
             @pl.loop(0, size // GROUP)
@@ -428,8 +442,8 @@
 
             far_part_copy(s, p).start()
 
-    def finish(j, which=None):
-        s = sources[j]
+    def finish(j, which=None, local=False):
+        s = source(j)
         base = side * 2 * cap + core * cap
         for p in count if which is None else which:
             if p == 0:
@@ -445,12 +459,12 @@
                     + near_part[s, 0, pl.ds(at, GROUP)].astype(jnp.float32)
                     + far_part[s, pl.ds(at, GROUP)].astype(jnp.float32)
                 ).astype(jnp.bfloat16)
-                if j == 0:
+                if local:
                     returned[s, pl.ds(at, GROUP)] = total
                 else:
                     result[s, pl.ds(at, GROUP)] = total
 
-            if j > 0:
+            if not local:
                 return_send(s, p).start()
 
     def gather_back(k):
@@ -515,7 +529,7 @@
         if ep > 1:
             pass_state()
 
-    own_group(0)
+    own_group(0, first=True)
     if line:
         arrive(1)
         relay(0)
@@ -524,12 +538,11 @@
 
         @pl.when(inner == 0)
         def _():
-            arrive(2, count[:1])
+            arrive(2, head)
             pl.semaphore_signal(
                 go_sem, inc=1, device_id={"ep": lax.rem(e + 2, ep)}, device_id_type=MESH
             )
-            arrive(2, count[1:])
-            start_send(3)
+            arrive(2, tail)
 
         @pl.when(inner == 1)
         def _():
@@ -543,6 +556,7 @@
 
         @pl.when(inner == 1)
         def _():
+            pair(1, head)
             arrive(2)
             pl.when(e == 1)(state_step)
 
@@ -552,21 +566,24 @@
         def _():
             pair(1)
             relay(2)
+            land(3)
+            start_send(3)
 
         @pl.when(inner == 1)
         def _():
-            arrive(3, count[:1])
+            arrive(3, head)
             relay(2)
-            arrive(3, count[1:])
+            arrive(3, tail)
 
         far_group(2)
 
         @pl.when(inner == 0)
         def _():
-            finish(1, count[:1])
+            finish(1, head)
             pair(2)
-            arrive(3)
-            finish(1, count[1:])
+            for p in count:
+                gather_start(source(3), p)
+            finish(1, tail)
 
         own_group(3)
 
@@ -580,7 +597,8 @@
         @pl.when(inner == 1)
         def _():
             pair(2)
-            finish(0)
+            finish(0, local=True)
+            finish(1, head)
             pl.when(e == 2)(state_step)
             relay(3)
 
@@ -592,22 +610,22 @@
 
         @pl.when(inner == 1)
         def _():
-            finish(2, count[:1])
+            finish(2, head)
             pair(3)
-            pair(1)
-            finish(2, count[1:])
+            pair(1, tail)
+            finish(2, tail)
 
         memory_part()
 
         @pl.when(inner == 0)
         def _():
-            finish(0)
+            finish(0, local=True)
             finish(3)
 
         @pl.when(inner == 1)
         def _():
             finish(3)
-            finish(1)
+            finish(1, tail)
 
         gather_back(0)
         gather_back(1)
@@ -615,19 +633,21 @@
         gather_back(2)
         gather_back(3)
     else:
-        for j in range(ep):
-            if j + 1 < ep:
-                arrive(j + 1)
-            if j > 0:
-                own_group(j)
+        relay(0)
+        far_group(0)
+        pair(0)
+        finish(0, local=True)
+
+        @pl.loop(1, ep)
+        def _(j):
+            arrive(j)
+            own_group(j)
             relay(j)
             far_group(j)
-            if j > 0:
-                pl.when(e == j)(state_step)
+            pl.when(e == j)(state_step)
             pair(j)
-            if j > 0:
-                finish(j - 1)
-        finish(ep - 1)
+            finish(j)
+
         memory_part()
         mix_part()
         for k in range(ep):
@@ -710,7 +730,7 @@
             square,
             square,
             square,
-            pltpu.VMEM((tiles, width, 2 * LANES), bf16),
+            pltpu.VMEM((width, 2 * part_hidden), bf16),
             pltpu.VMEM((part_hidden, width), bf16),
             pltpu.VMEM((ep, tp * cap, width), bf16),
             pltpu.VMEM((2 * cap, part_hidden), bf16),

time: 97.2 us -> 87 us (0.90)
  Pallas kernels: 92.9 us -> 82.7 us
    pallas_call x1, Pallas kernels: 92.9 us -> 82.7 us  [on_device(): pl.pallas_call(functools.partial(fused_kernel, ep, tp, cap), out_shape=(j...]
where the time goes in v2:
time: 87 us; the launch traced here: 86.8 us
  Pallas kernels  82.7 us (95%)
  local copies, waits for them, and re-layouts  3.45 us (4%)
    pallas_call x1, Pallas kernels, on_device(): pl.pallas_call(functools.partial(fused_kernel, ep, tp, cap), out_shape=(j...  82.7 us
    unnamed x2, local copies, waits for them, and re-layouts  3.45 us

profile of v2, /device:TPU:0, one launch (start us, length us, event | category | flops | bytes accessed | tf_op | source)
XLA Modules:
  0.0 86.8 jit_solution(295281140925718936)
XLA Ops:
  0.6 82.7 %shard_map.149 = (bf16[128,512]{1,0:T(8,128)(2,1)}, bf16[128,2048]{1,0:T(8,128)(2,1)}) custom-call(bf16[128,256]{1,0:T(8,128)(2,1)} %query_hbm.1, bf16[128,256]{1,0:T(8,128)(2,1)} %key_hbm.1, bf16[128,256]{1,0:T(8,128)(2,1)} %value_hbm.1, f32[2,128]{1,0:T(2,128)} %in_gate_ref.1, f32[2,128]{1,0:T(2,128)} %logit_ref.1, f32[2,128]{1,0:T(2,128)} %extra_ref.1, ...), custom_call_target="tpu_custom_call" | custom-call | flops 14092861440 | bytes 11010048 | tf_op jit(solution)/shard_map/pallas_call | solution.py:715
  83.3 1.6 %copy.18 = bf16[128,512]{1,0:T(8,128)(2,1)} copy(bf16[128,512]{1,0:T(8,128)(2,1)} %get-tuple-element.4) | data formatting | bytes 262144
  84.9 1.9 %copy.19 = bf16[128,2048]{1,0:T(8,128)(2,1)} copy(bf16[128,2048]{1,0:T(8,128)(2,1)} %get-tuple-element.5) | data formatting | bytes 1048576

commit v3 on v2

--- a/solution.py
+++ b/solution.py
@@ -20,8 +20,10 @@
 
 
 def pieces(cap):
-    first = cap // 32 * 16
-    return [(0, first), (first, cap - first)] if first else [(0, cap)]
+    step = cap // 32 * 16
+    if step == 0:
+        return [(0, cap)]
+    return [(at, min(step, cap - at)) for at in range(0, cap, step)]
 
 
 def fused_kernel(
@@ -31,14 +33,14 @@
     query_hbm,
     key_hbm,
     value_hbm,
-    in_gate_ref,
-    logit_ref,
-    extra_ref,
+    in_gate_hbm,
+    logit_hbm,
+    extra_hbm,
     mix_hbm,
     token_hbm,
-    gain_ref,
-    index_ref,
-    weight_ref,
+    gain_hbm,
+    index_hbm,
+    weight_hbm,
     gate_hbm,
     up_hbm,
     down_hbm,
@@ -47,6 +49,12 @@
     query_ref,
     key_ref,
     value_ref,
+    in_gate_ref,
+    logit_ref,
+    extra_ref,
+    gain_ref,
+    index_ref,
+    weight_ref,
     tokens,
     normed,
     send,
@@ -113,7 +121,7 @@
         def source(j):
             return sources[j]
 
-        gathers = [e, seat(3), seat(2), seat(1 - inner)]
+        gathers = [e, seat(3), seat(1 + inner), seat(2 - 2 * inner)]
     else:
         targets = [lax.rem(e + k, ep) for k in range(ep)]
         gathers = targets
@@ -159,7 +167,15 @@
         pltpu.make_async_copy(query_hbm, query_ref, own_sem.at[3]),
         pltpu.make_async_copy(key_hbm, key_ref, own_sem.at[4]),
         pltpu.make_async_copy(value_hbm, value_ref, own_sem.at[5]),
+        pltpu.make_async_copy(in_gate_hbm, in_gate_ref, own_sem.at[6]),
+        pltpu.make_async_copy(logit_hbm, logit_ref, own_sem.at[7]),
+        pltpu.make_async_copy(extra_hbm, extra_ref, own_sem.at[8]),
     ]
+    route_copies = [
+        pltpu.make_async_copy(index_hbm, index_ref, own_sem.at[9]),
+        pltpu.make_async_copy(weight_hbm, weight_ref, own_sem.at[10]),
+    ]
+    gain_copy = pltpu.make_async_copy(gain_hbm, gain_ref, own_sem.at[11])
 
     def z_send(s, p):
         return remote(
@@ -300,9 +316,11 @@
         memory_copy(0).start()
         memory_copy(1).start()
 
-    def mix_part():
+    def memory_relay():
         memory_copy(1).wait_recv()
         memory_copy(2).start()
+
+    def mix_part():
         mix_copy.wait()
         memory_copy(0).wait_recv()
         memory_copy(2).wait_recv()
@@ -342,12 +360,9 @@
         at_slot = lax.broadcasted_iota(jnp.int32, (cap, tok_rows), 0).astype(jnp.float32)
         taken = jnp.where(at_slot == slot_row[pl.ds(x, 1), :], 1.0, 0.0).astype(jnp.bfloat16)
 
-        @pl.loop(0, width // 512)
-        def _(i):
-            cols = pl.ds(pl.multiple_of(i * 512, 512), 512)
-            place[:, cols] = jnp.dot(
-                taken, normed[:, cols], preferred_element_type=jnp.float32
-            ).astype(jnp.bfloat16)
+        place[...] = jnp.dot(
+            taken, normed[...], preferred_element_type=jnp.float32
+        ).astype(jnp.bfloat16)
 
     def combine(x, first, last):
         lane = lax.broadcasted_iota(jnp.int32, (tok_rows, tok_rows), 1)
@@ -356,18 +371,13 @@
         at_slot = lax.broadcasted_iota(jnp.int32, (tok_rows, cap), 1).astype(jnp.float32)
         taken = jnp.where(at_slot == slot, 1.0, 0.0).astype(jnp.bfloat16)
 
-        @pl.loop(0, width // 512)
-        def _(i):
-            cols = pl.ds(pl.multiple_of(i * 512, 512), 512)
-            total = weight * jnp.dot(
-                taken, returned[x, :, cols], preferred_element_type=jnp.float32
-            )
-            if not first:
-                total = total + total_out[:, cols]
-            if last:
-                out_ref[:, cols] = total.astype(jnp.bfloat16)
-            else:
-                total_out[:, cols] = total
+        total = weight * jnp.dot(taken, returned[x], preferred_element_type=jnp.float32)
+        if not first:
+            total = total + total_out[...]
+        if last:
+            out_ref[...] = total.astype(jnp.bfloat16)
+        else:
+            total_out[...] = total
 
     def feed_forward(s, group, first=False):
         span = pl.ds(pl.multiple_of(group * 2 * cap, 2 * cap), 2 * cap)
@@ -467,17 +477,42 @@
             if not local:
                 return_send(s, p).start()
 
-    def gather_back(k):
+    def gather_back(k, first=False, last=False):
         x = gathers[k]
         if k > 0:
             for p in count:
                 return_recv(x, p).wait_recv()
-        combine(x, k == 0, k == ep - 1)
+        combine(x, first, last)
 
     def start_send(k):
         for p in count:
             z_send(targets[k], p).start()
 
+    def drain():
+        for i in range(3):
+            memory_copy(i).wait_send()
+
+        @pl.when(e + 1 < ep)
+        def _():
+            state_copy.wait_send()
+
+        @pl.loop(0, ep)
+        def _(s):
+            near_own_copy(s).wait_send()
+            near_far_copy(s).wait_send()
+            for p in count:
+                far_copy(s, p).wait_send()
+                near_copy(s, p).wait_send()
+                relay_copy(s, p).wait_send()
+                far_part_copy(s, p).wait_send()
+
+        @pl.loop(1, ep)
+        def _(k):
+            s = lax.rem(e + k, ep)
+            for p in count:
+                z_send(s, p).wait_send()
+                return_send(s, p).wait_send()
+
     def state_step():
         state_copy.wait_recv()
 
@@ -485,7 +520,10 @@
         def _():
             pass_state()
 
+    for copy in route_copies:
+        copy.start()
     token_copy.start()
+    gain_copy.start()
     for copy in head_copies:
         copy.start()
 
@@ -506,7 +544,10 @@
 
     for target in (near, far, across):
         pl.semaphore_signal(barrier, inc=1, device_id={"tp": target}, device_id_type=MESH)
+    for copy in route_copies:
+        copy.wait()
     slots()
+    gain_copy.wait()
     token_copy.wait()
     norm()
     dispatch(e, rows.at[e, block(side, core)])
@@ -546,7 +587,7 @@
 
         @pl.when(inner == 1)
         def _():
-            pair(0)
+            pair(0, count[:-1])
             pl.semaphore_wait(go_sem, 1)
             start_send(2)
             start_send(3)
@@ -556,9 +597,9 @@
 
         @pl.when(inner == 1)
         def _():
-            pair(1, head)
+            pair(1)
+            pl.when(e == 1)(state_step)
             arrive(2)
-            pl.when(e == 1)(state_step)
 
         own_group(2)
 
@@ -567,10 +608,11 @@
             pair(1)
             relay(2)
             land(3)
-            start_send(3)
+            pl.when(e > 0)(functools.partial(start_send, 3))
 
         @pl.when(inner == 1)
         def _():
+            pl.when(e == 2)(state_step)
             arrive(3, head)
             relay(2)
             arrive(3, tail)
@@ -579,6 +621,7 @@
 
         @pl.when(inner == 0)
         def _():
+            pl.when(e == 0)(functools.partial(start_send, 3))
             finish(1, head)
             pair(2)
             for p in count:
@@ -591,47 +634,45 @@
         def _():
             finish(2)
             pair(0)
-            pl.when(e == ep - 1)(state_step)
-            relay(3)
+            pl.when(e > 0)(state_step)
 
         @pl.when(inner == 1)
         def _():
             pair(2)
+            finish(1)
+            finish(0, count[:-1], local=True)
+
+        memory_part()
+        relay(3)
+        far_group(3)
+
+        @pl.when(inner == 0)
+        def _():
+            pair(3)
+            memory_relay()
             finish(0, local=True)
-            finish(1, head)
-            pl.when(e == 2)(state_step)
-            relay(3)
-
-        far_group(3)
-
-        @pl.when(inner == 0)
-        def _():
-            pair(3)
 
         @pl.when(inner == 1)
         def _():
             finish(2, head)
             pair(3)
-            pair(1, tail)
+            memory_relay()
+            pair(0, count[-1:])
             finish(2, tail)
 
-        memory_part()
-
-        @pl.when(inner == 0)
-        def _():
-            finish(0, local=True)
-            finish(3)
+        gather_back(1, first=True)
+        finish(3, head)
+        mix_part()
+        finish(3, tail)
 
         @pl.when(inner == 1)
         def _():
-            finish(3)
-            finish(1, tail)
+            finish(0, count[-1:], local=True)
 
         gather_back(0)
-        gather_back(1)
-        mix_part()
         gather_back(2)
-        gather_back(3)
+        drain()
+        gather_back(3, last=True)
     else:
         relay(0)
         far_group(0)
@@ -649,33 +690,11 @@
             finish(j)
 
         memory_part()
+        memory_relay()
         mix_part()
         for k in range(ep):
-            gather_back(k)
-
-    for i in range(3):
-        memory_copy(i).wait_send()
-
-    @pl.when(e + 1 < ep)
-    def _():
-        state_copy.wait_send()
-
-    @pl.loop(0, ep)
-    def _(s):
-        near_own_copy(s).wait_send()
-        near_far_copy(s).wait_send()
-        for p in count:
-            far_copy(s, p).wait_send()
-            near_copy(s, p).wait_send()
-            relay_copy(s, p).wait_send()
-            far_part_copy(s, p).wait_send()
-
-    @pl.loop(1, ep)
-    def _(k):
-        s = lax.rem(e + k, ep)
-        for p in count:
-            z_send(s, p).wait_send()
-            return_send(s, p).wait_send()
+            gather_back(k, k == 0, k == ep - 1)
+        drain()
 
 
 def on_device(
@@ -712,18 +731,25 @@
     slotted = pltpu.VMEM((ep, cap, width), bf16)
     head_rows = pltpu.VMEM(memory_query_rows.shape, bf16)
     token_rows = pltpu.VMEM((tok_rows, width), bf16)
+    head_gates = pltpu.VMEM(input_gate_log.shape, jnp.float32)
     return pl.pallas_call(
         functools.partial(fused_kernel, ep, tp, cap),
         out_shape=(
-            jax.ShapeDtypeStruct((positions, memory_output_weight.shape[1]), bf16),
-            jax.ShapeDtypeStruct((tok_rows, width), bf16),
+            pltpu.VMEM((positions, memory_output_weight.shape[1]), bf16),
+            pltpu.VMEM((tok_rows, width), bf16),
         ),
-        in_specs=[hbm] * 3 + [vmem] * 3 + [hbm] * 2 + [vmem] * 3 + [hbm] * 3,
+        in_specs=[hbm] * 14,
         out_specs=(vmem, vmem),
         scratch_shapes=[
             head_rows,
             head_rows,
             head_rows,
+            head_gates,
+            head_gates,
+            head_gates,
+            pltpu.VMEM((1, width), jnp.float32),
+            pltpu.VMEM((TOP, tok_rows), jnp.int32),
+            pltpu.VMEM((TOP, tok_rows), jnp.float32),
             token_rows,
             token_rows,
             slotted,
@@ -747,7 +773,7 @@
             pltpu.VMEM((tp, positions, heads * DH), bf16),
             pltpu.VMEM(memory_output_weight.shape, bf16),
             pltpu.SemaphoreType.DMA((2, tiles)),
-            pltpu.SemaphoreType.DMA((6,)),
+            pltpu.SemaphoreType.DMA((12,)),
             pltpu.SemaphoreType.DMA((2, 1)),
             split,
             split,

time: 87 us -> 76.8 us (0.88)
  Pallas kernels: 82.7 us -> 74.6 us
  local copies, waits for them, and re-layouts: 3.45 us -> 1.45 us
    pallas_call x1, Pallas kernels: 82.7 us -> 74.6 us  [on_device(): pl.pallas_call(functools.partial(fused_kernel, ep, tp, cap), out_shape=(p...]
    unnamed x2, local copies, waits for them, and re-layouts: 3.45 us -> 1.45 us
where the time goes in v3:
time: 76.8 us; the launch traced here: 76.7 us
  Pallas kernels  74.6 us (97%)
  local copies, waits for them, and re-layouts  1.45 us (2%)
    pallas_call x1, Pallas kernels, on_device(): pl.pallas_call(functools.partial(fused_kernel, ep, tp, cap), out_shape=(p...  74.6 us

profile of v3, /device:TPU:0, one launch (start us, length us, event | category | flops | bytes accessed | tf_op | source)
XLA Modules:
  0.0 76.7 jit_solution(16796038681563202526)
XLA Ops:
  0.6 74.6 %shard_map.149 = (bf16[128,512]{1,0:T(8,128)(2,1)S(1)}, bf16[128,2048]{1,0:T(8,128)(2,1)S(1)}) custom-call(bf16[128,256]{1,0:T(8,128)(2,1)} %query_hbm.1, bf16[128,256]{1,0:T(8,128)(2,1)} %key_hbm.1, bf16[128,256]{1,0:T(8,128)(2,1)} %value_hbm.1, f32[2,128]{1,0:T(2,128)} %in_gate_hbm.1, f32[2,128]{1,0:T(2,128)} %logit_hbm.1, f32[2,128]{1,0:T(2,128)} %extra_hbm.1, ...), custom_call_target="tpu_custom_call" | custom-call | flops 14092861440 | bytes 11010048 | tf_op jit(solution)/shard_map/pallas_call | solution.py:735
  75.2 0.7 copy.18
  75.9 0.8 %copy.19 = bf16[128,2048]{1,0:T(8,128)(2,1)} copy(bf16[128,2048]{1,0:T(8,128)(2,1)S(1)} %get-tuple-element.3) | data formatting | bytes 1048576

commit v4 on v3

--- a/solution.py
+++ b/solution.py
@@ -80,6 +80,7 @@
     w_sem,
     own_sem,
     st_sem,
+    sent_sem,
     z_sem,
     far_sem,
     near_sem,
@@ -89,7 +90,6 @@
     fp_sem,
     r_sem,
     m_sem,
-    go_sem,
 ):
     e = lax.axis_index("ep")
     t = lax.axis_index("tp")
@@ -106,6 +106,7 @@
     cuts = pieces(cap)
     count = range(len(cuts))
     head, tail = count[:1], count[1:]
+    most, last = count[:-1], count[-1:]
     line = ep == 4
 
     if line:
@@ -116,12 +117,12 @@
             return v * left + (3 - v) * (1 - left)
 
         targets = [e, seat(1 + 2 * inner), seat(3 - inner), seat(2 - 2 * inner)]
-        sources = [e, targets[3], targets[2], targets[1]]
+        sources = [e, seat(2 - 2 * inner), seat(1 + inner), seat(3)]
 
         def source(j):
             return sources[j]
 
-        gathers = [e, seat(3), seat(1 + inner), seat(2 - 2 * inner)]
+        gathers = [e, seat(1 + 2 * inner), seat(3 - inner), seat(2 - 2 * inner)]
     else:
         targets = [lax.rem(e + k, ep) for k in range(ep)]
         gathers = targets
@@ -180,57 +181,55 @@
     def z_send(s, p):
         return remote(
             send.at[s, cut(p)], rows.at[e, block(side, core, p)],
-            z_sem.at[0, s, p], z_sem.at[1, e, p], {"ep": s},
+            sent_sem.at[0], z_sem.at[e, p], {"ep": s},
         )
 
     def z_recv(s, p):
         return remote(
             send.at[s, cut(p)], rows.at[s, block(side, core, p)],
-            z_sem.at[0, s, p], z_sem.at[1, s, p], {"ep": s},
-        )
-
-    def mine_copy(s, p, sems, target):
+            sent_sem.at[0], z_sem.at[s, p], {"ep": s},
+        )
+
+    def far_copy(s, p):
         span = rows.at[s, block(side, core, p)]
-        return remote(span, span, sems.at[0, s, p], sems.at[1, s, p], {"tp": target})
-
-    def far_copy(s, p):
-        return mine_copy(s, p, far_sem, far)
+        return remote(span, span, sent_sem.at[1], far_sem.at[s, p], {"tp": far})
 
     def near_copy(s, p):
-        return mine_copy(s, p, near_sem, near)
+        span = rows.at[s, block(side, core, p)]
+        return remote(span, span, sent_sem.at[2], near_sem.at[s, p], {"tp": near})
 
     def relay_copy(s, p):
         span = rows.at[s, block(1 - side, core, p)]
-        return remote(span, span, relay_sem.at[0, s, p], relay_sem.at[1, s, p], {"tp": near})
+        return remote(span, span, sent_sem.at[3], relay_sem.at[s, p], {"tp": near})
 
     def near_own_copy(s):
         return remote(
             part.at[s, block(side, 1 - core)], near_part.at[s, 0],
-            no_sem.at[0, s], no_sem.at[1, s], {"tp": near},
+            sent_sem.at[4], no_sem.at[s], {"tp": near},
         )
 
     def near_far_copy(s):
         return remote(
             part.at[s, block(1 - side, 1 - core)], near_part.at[s, 1],
-            nf_sem.at[0, s], nf_sem.at[1, s], {"tp": near},
+            sent_sem.at[5], nf_sem.at[s], {"tp": near},
         )
 
     def far_part_copy(s, p):
         return remote(
             pair_sum.at[s, cut(p)], far_part.at[s, cut(p)],
-            fp_sem.at[0, s, p], fp_sem.at[1, s, p], {"tp": far},
+            sent_sem.at[6], fp_sem.at[s, p], {"tp": far},
         )
 
     def return_send(s, p):
         return remote(
             result.at[s, cut(p)], returned.at[e, cut(p)],
-            r_sem.at[0, s, p], r_sem.at[1, e, p], {"ep": s},
+            sent_sem.at[7], r_sem.at[e, p], {"ep": s},
         )
 
     def return_recv(s, p):
         return remote(
             result.at[s, cut(p)], returned.at[s, cut(p)],
-            r_sem.at[0, s, p], r_sem.at[1, s, p], {"ep": s},
+            sent_sem.at[7], r_sem.at[s, p], {"ep": s},
         )
 
     state_copy = remote(
@@ -349,7 +348,7 @@
         weight_col[...] = weights.T
 
     def norm():
-        @pl.loop(0, tok_rows // GROUP)
+        @pl.loop(0, tok_rows // GROUP, unroll=4)
         def _(i):
             span = pl.ds(pl.multiple_of(i * GROUP, GROUP), GROUP)
             values = tokens[span].astype(jnp.float32)
@@ -405,14 +404,17 @@
         far_copy(s, p).start()
         near_copy(s, p).start()
 
-    def land(j):
-        for p in count:
-            z_recv(source(j), p).wait_recv()
-
     def arrive(j, which=None):
         for p in count if which is None else which:
             z_recv(source(j), p).wait_recv()
             gather_start(source(j), p)
+
+    def weave(j, k):
+        for p in most:
+            arrive(j, [p])
+            relay(k, [p])
+        relay(k, last)
+        arrive(j, last)
 
     def own_group(j, first=False):
         s = source(j)
@@ -421,9 +423,9 @@
         feed_forward(s, side, first=first)
         near_own_copy(s).start()
 
-    def relay(j):
+    def relay(j, which=None):
         s = source(j)
-        for p in count:
+        for p in count if which is None else which:
             far_copy(s, p).wait_recv()
             relay_copy(s, p).start()
 
@@ -496,22 +498,13 @@
         def _():
             state_copy.wait_send()
 
-        @pl.loop(0, ep)
-        def _(s):
-            near_own_copy(s).wait_send()
-            near_far_copy(s).wait_send()
-            for p in count:
-                far_copy(s, p).wait_send()
-                near_copy(s, p).wait_send()
-                relay_copy(s, p).wait_send()
-                far_part_copy(s, p).wait_send()
-
-        @pl.loop(1, ep)
-        def _(k):
-            s = lax.rem(e + k, ep)
-            for p in count:
-                z_send(s, p).wait_send()
-                return_send(s, p).wait_send()
+        for k in range(8):
+            stages = ep - 1 if k in (0, 7) else ep
+            if stages:
+                span = send.at[pl.ds(0, stages)]
+                remote(
+                    span, span, sent_sem.at[k], no_sem.at[0], {"tp": near}
+                ).wait_send()
 
     def state_step():
         state_copy.wait_recv()
@@ -558,8 +551,8 @@
         dispatch(targets[k], send.at[targets[k]])
         if k == 1 or not line:
             start_send(k)
-        elif k == 2:
-            pl.when(inner == 0)(functools.partial(start_send, 2))
+        else:
+            pl.when(inner == 1)(functools.partial(start_send, k))
     for copy in head_copies:
         copy.wait()
     local_part()
@@ -572,105 +565,97 @@
 
     own_group(0, first=True)
     if line:
-        arrive(1)
-        relay(0)
+        weave(1, 0)
         far_group(0)
+        arrive(2, head)
         own_group(1)
 
         @pl.when(inner == 0)
         def _():
-            arrive(2, head)
-            pl.semaphore_signal(
-                go_sem, inc=1, device_id={"ep": lax.rem(e + 2, ep)}, device_id_type=MESH
-            )
-            arrive(2, tail)
-
-        @pl.when(inner == 1)
-        def _():
-            pair(0, count[:-1])
-            pl.semaphore_wait(go_sem, 1)
             start_send(2)
             start_send(3)
 
+        arrive(2, tail[:-1])
         relay(1)
+        arrive(2, last)
+        pl.when(e == 1)(state_step)
         far_group(1)
+        own_group(2)
+
+        @pl.when(inner == 0)
+        def _():
+            pair(1, head)
+            arrive(3, most)
+            relay(2)
+            arrive(3, last)
+            pair(1, tail)
 
         @pl.when(inner == 1)
-        def _():
-            pair(1)
-            pl.when(e == 1)(state_step)
-            arrive(2)
-
-        own_group(2)
-
-        @pl.when(inner == 0)
         def _():
             pair(1)
             relay(2)
-            land(3)
-            pl.when(e > 0)(functools.partial(start_send, 3))
+
+        far_group(2)
+
+        @pl.when(inner == 0)
+        def _():
+            finish(1, head)
 
         @pl.when(inner == 1)
         def _():
+            pair(2)
+            arrive(3)
+            finish(1)
+
+        own_group(3)
+
+        @pl.when(inner == 0)
+        def _():
+            pair(2, head)
+
+        @pl.when(inner == 1)
+        def _():
+            finish(2)
             pl.when(e == 2)(state_step)
-            arrive(3, head)
-            relay(2)
-            arrive(3, tail)
-
-        far_group(2)
+            memory_part()
+
+        relay(3)
+        pl.when(inner == 1)(functools.partial(pair, 0, most))
+        far_group(3)
 
         @pl.when(inner == 0)
         def _():
-            pl.when(e == 0)(functools.partial(start_send, 3))
-            finish(1, head)
-            pair(2)
-            for p in count:
-                gather_start(source(3), p)
             finish(1, tail)
-
-        own_group(3)
+            pair(3)
+            pair(2, tail)
+            finish(2, head)
+            pl.when(e > 2)(state_step)
+            memory_part()
+            pair(0, most)
+            finish(3)
+
+        @pl.when(inner == 1)
+        def _():
+            pair(3)
 
         @pl.when(inner == 0)
         def _():
-            finish(2)
-            pair(0)
-            pl.when(e > 0)(state_step)
+            pair(0, last)
+            finish(2, tail)
+
+        memory_relay()
+        gather_back(1, first=True)
+        mix_part()
 
         @pl.when(inner == 1)
         def _():
-            pair(2)
-            finish(1)
-            finish(0, count[:-1], local=True)
-
-        memory_part()
-        relay(3)
-        far_group(3)
-
-        @pl.when(inner == 0)
-        def _():
-            pair(3)
-            memory_relay()
-            finish(0, local=True)
-
-        @pl.when(inner == 1)
-        def _():
-            finish(2, head)
-            pair(3)
-            memory_relay()
-            pair(0, count[-1:])
-            finish(2, tail)
-
-        gather_back(1, first=True)
-        finish(3, head)
-        mix_part()
-        finish(3, tail)
-
-        @pl.when(inner == 1)
-        def _():
-            finish(0, count[-1:], local=True)
-
+            finish(3, most)
+            pair(0, last)
+            finish(3, last)
+
+        gather_back(2)
+        finish(0, local=True)
         gather_back(0)
-        gather_back(2)
         drain()
         gather_back(3, last=True)
     else:
@@ -724,8 +709,8 @@
     bf16 = jnp.bfloat16
     vmem = pl.BlockSpec(memory_space=pltpu.VMEM)
     hbm = pl.BlockSpec(memory_space=pl.ANY)
-    whole = pltpu.SemaphoreType.DMA((2, ep))
-    split = pltpu.SemaphoreType.DMA((2, ep, len(pieces(cap))))
+    whole = pltpu.SemaphoreType.DMA((ep,))
+    split = pltpu.SemaphoreType.DMA((ep, len(pieces(cap))))
     state = pltpu.VMEM((heads, DH + 8, DH), jnp.float32)
     square = pltpu.VMEM((tok_rows, tok_rows), jnp.float32)
     slotted = pltpu.VMEM((ep, cap, width), bf16)
@@ -775,6 +760,7 @@
             pltpu.SemaphoreType.DMA((2, tiles)),
             pltpu.SemaphoreType.DMA((12,)),
             pltpu.SemaphoreType.DMA((2, 1)),
+            pltpu.SemaphoreType.DMA((8,)),
             split,
             split,
             split,
@@ -784,7 +770,6 @@
             split,
             split,
             pltpu.SemaphoreType.DMA((2, 3)),
-            pltpu.SemaphoreType.REGULAR,
         ],
         compiler_params=pltpu.CompilerParams(
             collective_id=0, has_side_effects=True, vmem_limit_bytes=66000000

time: 76.8 us -> 73.9 us (0.962)
  Pallas kernels: 74.6 us -> 71.7 us
    pallas_call x1, Pallas kernels: 74.6 us -> 71.7 us  [on_device(): pl.pallas_call(functools.partial(fused_kernel, ep, tp, cap), out_shape=(p...]
where the time goes in v4:
time: 73.9 us; the launch traced here: 73.7 us
  Pallas kernels  71.7 us (97%)
  local copies, waits for them, and re-layouts  1.45 us (2%)
    pallas_call x1, Pallas kernels, on_device(): pl.pallas_call(functools.partial(fused_kernel, ep, tp, cap), out_shape=(p...  71.7 us

profile of v4, /device:TPU:0, one launch (start us, length us, event | category | flops | bytes accessed | tf_op | source)
XLA Modules:
  0.0 73.7 jit_solution(2347949882828041320)
XLA Ops:
  0.6 71.7 %shard_map.149 = (bf16[128,512]{1,0:T(8,128)(2,1)S(1)}, bf16[128,2048]{1,0:T(8,128)(2,1)S(1)}) custom-call(bf16[128,256]{1,0:T(8,128)(2,1)} %query_hbm.1, bf16[128,256]{1,0:T(8,128)(2,1)} %key_hbm.1, bf16[128,256]{1,0:T(8,128)(2,1)} %value_hbm.1, f32[2,128]{1,0:T(2,128)} %in_gate_hbm.1, f32[2,128]{1,0:T(2,128)} %logit_hbm.1, f32[2,128]{1,0:T(2,128)} %extra_hbm.1, ...), custom_call_target="tpu_custom_call" | custom-call | flops 14092861440 | bytes 11010048 | tf_op jit(solution)/shard_map/pallas_call | solution.py:720
  72.3 0.7 copy.18
  73.0 0.8 %copy.19 = bf16[128,2048]{1,0:T(8,128)(2,1)} copy(bf16[128,2048]{1,0:T(8,128)(2,1)S(1)} %get-tuple-element.3) | data formatting | bytes 1048576

commit v5 on v4

--- a/solution.py
+++ b/solution.py
@@ -107,7 +107,7 @@
     count = range(len(cuts))
     head, tail = count[:1], count[1:]
     most, last = count[:-1], count[-1:]
-    line = ep == 4
+    line = ep == 4 and len(cuts) > 1
 
     if line:
         left = 1 - e // 2
@@ -208,10 +208,17 @@
             sent_sem.at[4], no_sem.at[s], {"tp": near},
         )
 
-    def near_far_copy(s):
+    def stretch(which):
+        start = cuts[which[0]][0]
+        return start, sum(cuts[p][1] for p in which)
+
+    def near_far_copy(s, which):
+        start, size = stretch(which)
+        base = ((1 - side) * 2 + 1 - core) * cap + start
         return remote(
-            part.at[s, block(1 - side, 1 - core)], near_part.at[s, 1],
-            sent_sem.at[5], nf_sem.at[s], {"tp": near},
+            part.at[s, pl.ds(pl.multiple_of(base, GROUP), size)],
+            near_part.at[s, 1, pl.ds(start, size)],
+            sent_sem.at[5], nf_sem.at[s, which[0]], {"tp": near},
         )
 
     def far_part_copy(s, p):
@@ -378,9 +385,11 @@
         else:
             total_out[...] = total
 
-    def feed_forward(s, group, first=False):
-        span = pl.ds(pl.multiple_of(group * 2 * cap, 2 * cap), 2 * cap)
+    def feed_forward(s, spans, first=False):
+        size = sum(span.size for span in spans)
         step = 4 * LANES
+        if len(spans) > 1:
+            taken = jnp.concatenate([rows[s, span] for span in spans], axis=0)
         for start in range(0, 2 * part_hidden, step):
             stop = min(start + step, 2 * part_hidden)
             if first:
@@ -388,17 +397,27 @@
                     for copy in weight_copies(i):
                         copy.wait()
             both = jnp.dot(
-                rows[s, span], gate_up[:, start:stop], preferred_element_type=jnp.float32
+                taken if len(spans) > 1 else rows[s, spans[0]], gate_up[:, start:stop],
+                preferred_element_type=jnp.float32,
             )
             for i in range(0, stop - start, 2 * LANES):
                 act, up_act = both[:, i : i + LANES], both[:, i + LANES : i + 2 * LANES]
                 at = (start + i) // 2
-                hidden[:, at : at + LANES] = (jax.nn.silu(act) * up_act).astype(jnp.bfloat16)
+                hidden[0:size, at : at + LANES] = (
+                    jax.nn.silu(act) * up_act
+                ).astype(jnp.bfloat16)
         if first:
             down_copy.wait()
-        part[s, span] = jnp.dot(
-            hidden[...], down[...], preferred_element_type=jnp.float32
+        made = jnp.dot(
+            hidden[0:size], down[...], preferred_element_type=jnp.float32
         ).astype(jnp.bfloat16)
+        done = 0
+        for span in spans:
+            part[s, span] = made[done : done + span.size]
+            done += span.size
+
+    def chip_rows(group):
+        return pl.ds(pl.multiple_of(group * 2 * cap, 2 * cap), 2 * cap)
 
     def gather_start(s, p):
         far_copy(s, p).start()
@@ -420,7 +439,7 @@
         s = source(j)
         for p in count:
             near_copy(s, p).wait_recv()
-        feed_forward(s, side, first=first)
+        feed_forward(s, [chip_rows(side)], first=first)
         near_own_copy(s).start()
 
     def relay(j, which=None):
@@ -433,15 +452,28 @@
         s = source(j)
         for p in count:
             relay_copy(s, p).wait_recv()
-        feed_forward(s, 1 - side)
-        near_far_copy(s).start()
-
-    def pair(j, which=None):
+        feed_forward(s, [chip_rows(1 - side)])
+        near_far_copy(s, count).start()
+
+    def far_cut(j, which):
+        s = source(j)
+        for p in which:
+            relay_copy(s, p).wait_recv()
+        start, size = stretch(which)
+        base = (1 - side) * 2 * cap + start
+        feed_forward(
+            s, [pl.ds(pl.multiple_of(base + c * cap, GROUP), size) for c in range(2)]
+        )
+        near_far_copy(s, which).start()
+
+    def pair(j, which=None, cut_at=None):
         s = source(j)
         base = (1 - side) * 2 * cap + core * cap
         for p in count if which is None else which:
             if p == 0:
-                near_far_copy(s).wait_recv()
+                near_far_copy(s, count if cut_at is None else count[:cut_at]).wait_recv()
+            elif p == cut_at:
+                near_far_copy(s, count[cut_at:]).wait_recv()
             off, size = cuts[p]
 
             @pl.loop(0, size // GROUP)
@@ -619,39 +651,36 @@
             pl.when(e == 2)(state_step)
             memory_part()
 
-        relay(3)
-        pl.when(inner == 1)(functools.partial(pair, 0, most))
-        far_group(3)
+        relay(3, head)
+        far_cut(3, head)
+        pl.when(inner == 1)(functools.partial(pair, 0, head))
+        relay(3, tail)
+        pair(3, head, cut_at=1)
+        far_cut(3, tail)
 
         @pl.when(inner == 0)
         def _():
             finish(1, tail)
-            pair(3)
+            pair(3, tail, cut_at=1)
             pair(2, tail)
             finish(2, head)
             pl.when(e > 2)(state_step)
             memory_part()
             pair(0, most)
             finish(3)
-
-        @pl.when(inner == 1)
-        def _():
-            pair(3)
-
-        @pl.when(inner == 0)
-        def _():
             pair(0, last)
             finish(2, tail)
 
+        pl.when(inner == 1)(functools.partial(pair, 3, tail, 1))
         memory_relay()
         gather_back(1, first=True)
         mix_part()
 
         @pl.when(inner == 1)
         def _():
-            finish(3, most)
-            pair(0, last)
-            finish(3, last)
+            finish(3, head)
+            pair(0, tail)
+            finish(3, tail)
 
         gather_back(2)
         finish(0, local=True)
@@ -766,7 +795,7 @@
             split,
             split,
             whole,
-            whole,
+            split,
             split,
             split,
             pltpu.SemaphoreType.DMA((2, 3)),

time: 73.9 us -> 71.8 us (0.972)
  Pallas kernels: 71.7 us -> 69.5 us
    pallas_call x1, Pallas kernels: 71.7 us -> 69.5 us  [on_device(): pl.pallas_call(functools.partial(fused_kernel, ep, tp, cap), out_shape=(p...]
where the time goes in v5:
time: 71.8 us; the launch traced here: 71.6 us
  Pallas kernels  69.5 us (97%)
  local copies, waits for them, and re-layouts  1.45 us (2%)
    pallas_call x1, Pallas kernels, on_device(): pl.pallas_call(functools.partial(fused_kernel, ep, tp, cap), out_shape=(p...  69.5 us
    unnamed x2, local copies, waits for them, and re-layouts  1.45 us

profile of v5, /device:TPU:0, one launch (start us, length us, event | category | flops | bytes accessed | tf_op | source)
XLA Modules:
  0.0 71.6 jit_solution(5371333081997339143)
XLA Ops:
  0.6 69.5 %shard_map.149 = (bf16[128,512]{1,0:T(8,128)(2,1)S(1)}, bf16[128,2048]{1,0:T(8,128)(2,1)S(1)}) custom-call(bf16[128,256]{1,0:T(8,128)(2,1)} %query_hbm.1, bf16[128,256]{1,0:T(8,128)(2,1)} %key_hbm.1, bf16[128,256]{1,0:T(8,128)(2,1)} %value_hbm.1, f32[2,128]{1,0:T(2,128)} %in_gate_hbm.1, f32[2,128]{1,0:T(2,128)} %logit_hbm.1, f32[2,128]{1,0:T(2,128)} %extra_hbm.1, ...), custom_call_target="tpu_custom_call" | custom-call | flops 14092861440 | bytes 11010048 | tf_op jit(solution)/shard_map/pallas_call | solution.py:749
  70.2 0.7 copy.18
  70.8 0.8 %copy.19 = bf16[128,2048]{1,0:T(8,128)(2,1)} copy(bf16[128,2048]{1,0:T(8,128)(2,1)S(1)} %get-tuple-element.3) | data formatting | bytes 1048576
